TPU v7x, 32 devices: a whole 2x2x4 slice. The times are simulated.
32 devices in a mesh: gr: 2 (over x), fs: 8 (over z, y), tp: 2 (over core).
Axes of the slice: x: 2, y: 2, z: 4, core: 2. Of those that a mesh axis runs over, the one named last changes fastest.
Arguments:
- tokens: bfloat16 [4096, 2048], P(('gr', 'fs', 'tp')), may hold values from -6 to 6
- routes: int32 [4096, 8], P(('gr', 'fs', 'tp')), may hold values from 0 to 15, all different within a row; in each aligned block of 128 rows (0 to 127, 128 to 255, ...) at most 96 rows name the same one
- route_weights: float32 [4096, 8], P(('gr', 'fs', 'tp')), may hold values from 0.1 to 0.6
- norm_gain: float32 [2048], P(('gr', 'tp')), may hold values from 0.1 to 1.9
- gate_trained: float32 [16, 384, 2048], P(None, 'fs', ('gr', 'tp')), may hold values from -0.125 to 0.125
- up_trained: float32 [16, 384, 2048], P(None, 'fs', ('gr', 'tp')), may hold values from -0.125 to 0.125
- down_trained: float32 [16, 384, 2048], P(None, 'fs', ('gr', 'tp')), may hold values from -0.3125 to 0.3125
- shared_gate_trained: float32 [512, 2048], P('fs', ('gr', 'tp')), may hold values from -0.125 to 0.125
- shared_up_trained: float32 [512, 2048], P('fs', ('gr', 'tp')), may hold values from -0.125 to 0.125
- shared_down_trained: float32 [512, 2048], P('fs', ('gr', 'tp')), may hold values from -0.25 to 0.25
Outputs:
- combined: bfloat16 [4096, 2048], P(('gr', 'fs', 'tp'))
- expert_gate: bfloat16 [16, 384, 2048], P(('fs', 'tp'))
- expert_up: bfloat16 [16, 384, 2048], P(('fs', 'tp'))
- expert_down: bfloat16 [16, 384, 2048], P(('fs', 'tp'))
- shared_gate: bfloat16 [512, 2048], P('fs')
- shared_up: bfloat16 [512, 2048], P('fs')
- shared_down: bfloat16 [512, 2048], P('fs')
Inputs may be any that keep to these rules, and one draw needn't show every extreme that they name: `routes`: each row names 8 different experts. Among the rows of one device no expert is named more than 96 times, and that many is reached in every draw.
All inputs are finite; a program needn't handle non-finite values.
Results may differ from a plain program's by a relative error of at most 0.0084.
Values may be sent and summed in bfloat16 or wider, within the bound.
A program may use at most 128 MiB of HBM per device.

v0:
```python
import functools

import jax
import jax.numpy as jnp
from jax import lax
from jax.experimental import pallas as pl
from jax.experimental.pallas import tpu as pltpu
from jax.sharding import PartitionSpec as P

epsilon = 1e-06
LANES = 128
MESH = pl.DeviceIdType.MESH


def contract_rows(inputs, matrix):
    return lax.dot_general(
        inputs, matrix, (((1,), (1,)), ((), ())), preferred_element_type=jnp.float32
    )


def swiglu_rows(inputs, gate_matrix, up_matrix, down_matrix):
    hidden = (
        jax.nn.silu(contract_rows(inputs, gate_matrix)) * contract_rows(inputs, up_matrix)
    ).astype(jnp.bfloat16)
    return jnp.dot(hidden, down_matrix, preferred_element_type=jnp.float32)


def dispatch_body(
    tokens,
    routes,
    route_weights,
    norm_gain,
    gate_trained,
    up_trained,
    down_trained,
    shared_gate_trained,
    shared_up_trained,
    shared_down_trained,
):
    gain_row = norm_gain[None, None, :]
    stacked = jnp.stack(
        [gate_trained * gain_row, up_trained * gain_row, down_trained], axis=1
    ).astype(jnp.bfloat16)
    halves = lax.all_to_all(
        lax.all_to_all(stacked[:, :, :, None, :], "fs", split_axis=0, concat_axis=2, tiled=True),
        "tp",
        split_axis=0,
        concat_axis=3,
        tiled=True,
    )
    owned = lax.all_gather(halves[:, :, :, None], "gr", axis=3, tiled=True)
    owned = owned.reshape(owned.shape[0], 3, owned.shape[2], -1)
    expert_gate = owned[:, 0]
    expert_up = owned[:, 1]
    expert_down = owned[:, 2]
    shared_gain = norm_gain[None, :]
    shared_stack = jnp.stack(
        [shared_gate_trained * shared_gain, shared_up_trained * shared_gain, shared_down_trained],
        axis=0,
    ).astype(jnp.bfloat16)
    shared_whole = lax.all_gather(shared_stack, ("gr", "tp"), axis=2, tiled=True)
    shared_gate = shared_whole[0]
    shared_up = shared_whole[1]
    shared_down = shared_whole[2]
    values = tokens.astype(jnp.float32)
    normed = (
        values * lax.rsqrt(jnp.mean(values * values, axis=1, keepdims=True) + epsilon)
    ).astype(jnp.bfloat16)
    row_count, features = normed.shape
    per_token = routes.shape[1]
    shared_out = swiglu_rows(
        normed,
        lax.all_gather(shared_gate, "fs", axis=0, tiled=True),
        lax.all_gather(shared_up, "fs", axis=0, tiled=True),
        lax.all_gather(shared_down, "fs", axis=0, tiled=True),
    )
    experts = lax.axis_size("fs") * lax.axis_size("tp")
    capacity = max(2, 3 * row_count * per_token // (2 * experts))
    chosen = routes.reshape(-1)
    onehot = (chosen[:, None] == jnp.arange(experts, dtype=jnp.int32)[None, :]).astype(jnp.int32)
    position = jnp.sum((jnp.cumsum(onehot, axis=0) - onehot) * onehot, axis=1)
    target = chosen * capacity + position
    source = (
        jnp.full((experts * capacity,), row_count, jnp.int32)
        .at[target]
        .set(jnp.arange(row_count * per_token, dtype=jnp.int32) // per_token)
    )
    padded = jnp.concatenate([normed, jnp.zeros((1, features), jnp.bfloat16)], axis=0)
    outgoing = padded[source].reshape(experts, capacity, features)
    arrived = lax.all_to_all(outgoing, ("fs", "tp"), split_axis=0, concat_axis=0, tiled=True)
    item_count = arrived.shape[1]
    result = swiglu_rows(
        arrived.reshape(-1, features), expert_gate[0], expert_up[0], expert_down[0]
    )
    result = result.astype(jnp.bfloat16).reshape(experts, item_count, features)
    returned = lax.all_to_all(result, ("fs", "tp"), split_axis=0, concat_axis=0, tiled=True)
    picked = returned.reshape(experts * capacity, features)[target].astype(jnp.float32)
    picked = picked.reshape(row_count, per_token, features)
    routed = jnp.sum(picked * route_weights[:, :, None], axis=1)
    combined = (routed + shared_out).astype(jnp.bfloat16)
    return (combined, expert_gate, expert_up, expert_down, shared_gate, shared_up, shared_down)


def exchange_kernel(
    n,
    pieces_ref,
    shared_ref,
    rows_ref,
    combined_ref,
    gate_ref,
    up_ref,
    down_ref,
    shared_gate_ref,
    shared_up_ref,
    shared_down_ref,
    weights,
    shared,
    rows,
    parts,
    pair_in,
    sums,
    side_in,
    sums_in,
    local_sem,
    piece_sem,
    weight_sem,
    column_out_sem,
    column_sem,
    shared_out_sem,
    shared_sem,
    row_out_sem,
    row_side_sem,
    row_back_sem,
    row_sem,
    row_pair_out_sem,
    row_pair_sem,
    part_sem,
    part_recv_sem,
    side_sem,
    side_recv_sem,
    sum_sem,
    sum_recv_sem,
    out_sem,
):
    gr, fs, tp = lax.axis_index("gr"), lax.axis_index("fs"), lax.axis_index("tp")
    other = 1 - tp
    across = (1 - gr, fs, tp)
    twin = (gr, fs, other)
    expert = fs * 2 + tp
    hidden_piece, width = pieces_ref.shape[2], pieces_ref.shape[3]
    hidden = n * hidden_piece
    shared_piece = shared_ref.shape[1]
    extra = shared_piece // 2
    features = 4 * width
    row_count = rows_ref.shape[0]
    depth = n // 2
    outer, inner = lax.div(fs, 2), lax.rem(fs, 2)
    beside = (gr, outer * 2 + 1 - inner, tp)

    barrier = pltpu.get_barrier_semaphore()
    pl.semaphore_signal(barrier, inc=1, device_id=across, device_id_type=MESH)
    pl.semaphore_signal(barrier, inc=1, device_id=twin, device_id_type=MESH)
    for k in range(1, n):
        for t in range(2):
            pl.semaphore_signal(
                barrier, inc=1, device_id=(gr, lax.rem(fs + k, n), t), device_id_type=MESH
            )
    pl.semaphore_wait(barrier, 2 * n)

    def remote(src, dst, send, recv, device):
        return pltpu.make_async_remote_copy(
            src_ref=src,
            dst_ref=dst,
            send_sem=send,
            recv_sem=recv,
            device_id=device,
            device_id_type=MESH,
        )

    def columns(g, t):
        return pl.ds(pl.multiple_of((g * 2 + t) * width, width), width)

    def slab(source, span):
        start = pl.multiple_of(source * hidden_piece, 16)
        return weights.at[:, pl.ds(start, hidden_piece), span]

    def row_block(source, t):
        start = pl.multiple_of((source * 2 + t) * row_count, row_count)
        return rows.at[pl.ds(start, row_count)]

    half = pl.ds(pl.multiple_of(gr * 2 * width, width), 2 * width)
    far_half = pl.ds(pl.multiple_of((1 - gr) * 2 * width, width), 2 * width)

    def piece_send(d, t):
        return remote(
            pieces_ref.at[d * 2 + t],
            slab(fs, columns(gr, tp)),
            piece_sem.at[d, t],
            weight_sem.at[fs, tp],
            (gr, d, t),
        )

    def column_send(source):
        return remote(slab(source, half), slab(source, half), column_out_sem.at[source], column_sem.at[source], across)

    def row_move(source, send, recv, device):
        return remote(row_block(source, tp), row_block(source, tp), send, recv, device)

    def row_onward(source, step):
        return row_move(
            source,
            row_out_sem.at[source],
            row_sem.at[source],
            (gr, (outer + step) * 2 + inner, tp),
        )

    def row_beside(source):
        return row_move(source, row_side_sem.at[lax.div(source, 2)], row_sem.at[source], beside)

    def row_relay(source):
        return row_move(source, row_pair_out_sem.at[source], row_pair_sem.at[source], twin)

    def row_back():
        return row_move(
            fs, row_back_sem.at[0], row_sem.at[fs], (gr, (outer - 1) * 2 + inner, tp)
        )

    def at_distance(action):
        for distance in range(1, depth):
            for step in (1, -1):
                place = outer - step * distance

                @pl.when((place >= 0) & (place < depth))
                def _():
                    action(place, step)

    def onward_exists(step):
        return (outer + step >= 0) & (outer + step < depth)

    own_piece = pltpu.make_async_copy(
        pieces_ref.at[expert], slab(fs, columns(gr, tp)), local_sem.at[0]
    )
    own_shared = pltpu.make_async_copy(
        shared_ref, shared.at[:, :, columns(gr, tp)], local_sem.at[1]
    )
    own_rows = pltpu.make_async_copy(rows_ref, row_block(fs, tp), local_sem.at[2])
    own_rows.start()
    own_piece.start()
    own_shared.start()
    own_rows.wait()

    @pl.when(outer < depth - 1)
    def _():
        row_onward(fs, 1).start()

    @pl.when(outer > 0)
    def _():
        row_back().start()

    row_beside(fs).start()
    row_relay(fs).start()

    twin_piece = piece_send(fs, other)
    twin_piece.start()
    shared_far = remote(
        shared_ref, shared.at[:, :, columns(gr, tp)], shared_out_sem.at[0], shared_sem.at[0], across
    )
    shared_far.start()
    shared_twin = remote(
        shared_ref, shared.at[:, :, columns(gr, tp)], shared_out_sem.at[1], shared_sem.at[1], twin
    )
    shared_twin.start()

    for k in range(1, n):
        d = lax.rem(fs + k, n)
        piece_send(d, 0).start()
        piece_send(d, 1).start()
    own_piece.wait()
    twin_arrival = remote(
        pieces_ref.at[0], slab(fs, columns(gr, other)), piece_sem.at[fs, other], weight_sem.at[fs, other], twin
    )
    twin_arrival.wait_recv()
    column_send(fs).start()

    def take_rows(source):
        row_move(source, row_out_sem.at[source], row_sem.at[source], twin).wait_recv()

    def take_weights(source):
        for t in range(2):
            remote(
                pieces_ref.at[0],
                slab(source, columns(gr, t)),
                piece_sem.at[fs, other],
                weight_sem.at[source, t],
                twin,
            ).wait_recv()
        column_send(source).start()

    def arrive(place, step):
        source = place * 2 + inner
        take_rows(source)

        @pl.when(onward_exists(step))
        def _():
            row_onward(source, step).start()

        row_beside(source).start()
        row_relay(source).start()
        take_weights(source)
        take_weights(place * 2 + 1 - inner)

    def arrive_beside(place, step):
        source = place * 2 + 1 - inner
        take_rows(source)
        row_relay(source).start()

    take_weights(outer * 2 + 1 - inner)
    at_distance(arrive)
    arrive_beside(outer, 0)
    at_distance(arrive_beside)

    own_shared.wait()
    far_columns = shared.at[:, :, columns(1 - gr, tp)]
    remote(shared_ref, far_columns, shared_out_sem.at[0], shared_sem.at[0], across).wait_recv()
    shared_relay = remote(far_columns, far_columns, shared_out_sem.at[2], shared_sem.at[2], twin)
    shared_relay.start()
    remote(
        shared_ref, shared.at[:, :, columns(gr, other)], shared_out_sem.at[1], shared_sem.at[1], twin
    ).wait_recv()
    last_columns = shared.at[:, :, columns(1 - gr, other)]
    remote(shared_ref, last_columns, shared_out_sem.at[2], shared_sem.at[2], twin).wait_recv()
    tail = pltpu.make_async_copy(
        shared.at[:, pl.ds(pl.multiple_of(tp * extra, extra), extra), :],
        weights.at[:, pl.ds(hidden, extra), :],
        local_sem.at[3],
    )
    tail.start()

    for k in range(n):
        source = lax.rem(fs + n - k, n)
        remote(
            slab(source, far_half),
            slab(source, far_half),
            column_out_sem.at[source],
            column_sem.at[source],
            across,
        ).wait_recv()
    tail.wait()
    outs = []
    for j, ref in enumerate((gate_ref, up_ref, down_ref)):
        outs.append(
            pltpu.make_async_copy(weights.at[j, pl.ds(0, hidden), :], ref.at[0], out_sem.at[j])
        )
    for j, ref in enumerate((shared_gate_ref, shared_up_ref, shared_down_ref)):
        outs.append(pltpu.make_async_copy(shared.at[j], ref, out_sem.at[3 + j]))
    for copy in outs:
        copy.start()

    def part_send(k):
        return pltpu.make_async_remote_copy(
            src_ref=parts.at[k, pl.ds(pl.multiple_of(other * row_count, row_count), row_count), :],
            dst_ref=pair_in.at[k],
            send_sem=part_sem.at[k],
            recv_sem=part_recv_sem.at[k],
            device_id=twin,
            device_id_type=MESH,
        )

    def place_of(k):
        return lax.rem(outer + 1 + lax.rem(k, depth), depth)

    def side_send(k):
        return pltpu.make_async_remote_copy(
            src_ref=sums.at[k],
            dst_ref=side_in.at[k],
            send_sem=side_sem.at[k],
            recv_sem=side_recv_sem.at[k],
            device_id=beside,
            device_id_type=MESH,
        )

    def sum_send(k):
        return pltpu.make_async_remote_copy(
            src_ref=sums.at[k],
            dst_ref=sums_in.at[k - depth],
            send_sem=sum_sem.at[k - depth],
            recv_sem=sum_recv_sem.at[k - depth],
            device_id=(gr, place_of(k) * 2 + inner, tp),
            device_id_type=MESH,
        )

    chunk = 32

    def add_pair(k):
        part_send(k).wait_recv()

        @pl.loop(0, row_count // chunk)
        def _(i):
            at = pl.multiple_of(i * chunk, chunk)
            mine = pl.multiple_of(tp * row_count + i * chunk, chunk)
            value = parts[k, pl.ds(mine, chunk), :].astype(jnp.float32)
            value = value + pair_in[k, pl.ds(at, chunk), :].astype(jnp.float32)
            sums[k, pl.ds(at, chunk), :] = value.astype(jnp.bfloat16)

    def add_both(k):
        part_send(k).wait_recv()
        side_send(k - depth).wait_recv()

        @pl.loop(0, row_count // chunk)
        def _(i):
            at = pl.multiple_of(i * chunk, chunk)
            mine = pl.multiple_of(tp * row_count + i * chunk, chunk)
            value = parts[k, pl.ds(mine, chunk), :].astype(jnp.float32)
            value = value + pair_in[k, pl.ds(at, chunk), :].astype(jnp.float32)
            value = value + side_in[k - depth, pl.ds(at, chunk), :].astype(jnp.float32)
            sums[k, pl.ds(at, chunk), :] = value.astype(jnp.bfloat16)

    @pl.loop(0, n)
    def _(k):
        d = place_of(k) * 2 + jnp.where(k < depth, 1 - inner, inner)
        remote(
            row_block(d, other), row_block(d, other), row_pair_out_sem.at[d], row_pair_sem.at[d], twin
        ).wait_recv()
        block = pl.ds(pl.multiple_of(d * 2 * row_count, 2 * row_count), 2 * row_count)
        inputs = rows[block, 0:features]
        factors = rows[block, features : features + LANES].astype(jnp.float32)
        lane = lax.broadcasted_iota(jnp.int32, factors.shape, 1)
        chosen = (lane == expert) | (lane == expert + LANES // 2)
        factor = jnp.sum(jnp.where(chosen, factors, 0.0), axis=1, keepdims=True)
        gate = contract_rows(inputs, weights[0])
        up = contract_rows(inputs, weights[1])
        unit = lax.broadcasted_iota(jnp.int32, gate.shape, 1)
        scale = jnp.where(unit < hidden, factor, 1.0)
        units = (gate / (1.0 + jnp.exp(-gate)) * up * scale).astype(jnp.bfloat16)
        for c in range(4):
            span = pl.ds(c * width, width)
            parts[k, :, span] = jnp.dot(
                units, weights[2, :, span], preferred_element_type=jnp.float32
            ).astype(jnp.bfloat16)
        part_send(k).start()

        @pl.when((k > 0) & (k <= depth))
        def _():
            add_pair(k - 1)
            side_send(k - 1).start()

        @pl.when(k > depth)
        def _():
            add_both(k - 1)
            sum_send(k - 1).start()

    add_both(n - 1)
    for k in range(depth, n - 1):
        sum_send(k).wait_recv()

    @pl.loop(0, row_count // chunk)
    def _(i):
        at = pl.ds(pl.multiple_of(i * chunk, chunk), chunk)
        total = sums[n - 1, at, :].astype(jnp.float32)
        for k in range(depth - 1):
            total = total + sums_in[k, at, :].astype(jnp.float32)
        combined_ref[at, :] = total.astype(jnp.bfloat16)

    twin_piece.wait_send()
    shared_far.wait_send()
    shared_twin.wait_send()
    shared_relay.wait_send()
    row_relay(fs).wait_send()
    row_beside(fs).wait_send()

    @pl.when(outer < depth - 1)
    def _():
        row_onward(fs, 1).wait_send()

    @pl.when(outer > 0)
    def _():
        row_back().wait_send()

    def sent(place, step):
        source = place * 2 + inner

        @pl.when(onward_exists(step))
        def _():
            row_onward(source, step).wait_send()

        row_beside(source).wait_send()

    at_distance(sent)
    column_send(fs).wait_send()
    for k in range(1, n):
        piece_send(lax.rem(fs + k, n), 0).wait_send()
        piece_send(lax.rem(fs + k, n), 1).wait_send()
        column_send(lax.rem(fs + k, n)).wait_send()
        row_relay(lax.rem(fs + k, n)).wait_send()
    for k in range(n):
        part_send(k).wait_send()
    for k in range(depth):
        side_send(k).wait_send()
    for k in range(depth, n - 1):
        sum_send(k).wait_send()
    for copy in outs:
        copy.wait()


def direct_body(
    tokens,
    routes,
    route_weights,
    norm_gain,
    gate_trained,
    up_trained,
    down_trained,
    shared_gate_trained,
    shared_up_trained,
    shared_down_trained,
):
    gain_row = norm_gain[None, None, :]
    pieces = jnp.stack(
        [gate_trained * gain_row, up_trained * gain_row, down_trained], axis=1
    ).astype(jnp.bfloat16)
    shared_gain = norm_gain[None, :]
    shared_stack = jnp.stack(
        [shared_gate_trained * shared_gain, shared_up_trained * shared_gain, shared_down_trained],
        axis=0,
    ).astype(jnp.bfloat16)
    values = tokens.astype(jnp.float32)
    normed = (
        values * lax.rsqrt(jnp.mean(values * values, axis=1, keepdims=True) + epsilon)
    ).astype(jnp.bfloat16)
    n = lax.axis_size("fs")
    experts, _, hidden_piece, width = pieces.shape
    row_count, features = normed.shape
    shared_piece = shared_stack.shape[1]
    numbers = jnp.arange(LANES // 2, dtype=jnp.int32)
    factors = jnp.sum(
        jnp.where(routes[:, :, None] == numbers, route_weights[:, :, None], 0.0), axis=1
    )
    high = lax.reduce_precision(factors, 8, 7)
    rows = jnp.concatenate(
        [normed, high.astype(jnp.bfloat16), (factors - high).astype(jnp.bfloat16)], axis=1
    )
    hidden = n * hidden_piece
    hidden_all = hidden + shared_piece // 2
    vmem = pl.BlockSpec(memory_space=pltpu.VMEM)
    hbm = pl.BlockSpec(memory_space=pl.ANY)
    kind = jnp.bfloat16
    expert_shape = jax.ShapeDtypeStruct((1, hidden, features), kind)
    shared_shape = jax.ShapeDtypeStruct((shared_piece, features), kind)
    DMA = pltpu.SemaphoreType.DMA
    return pl.pallas_call(
        functools.partial(exchange_kernel, n),
        out_shape=(jax.ShapeDtypeStruct((row_count, features), kind),)
        + (expert_shape,) * 3
        + (shared_shape,) * 3,
        in_specs=[vmem] * 3,
        out_specs=(vmem,) + (hbm,) * 6,
        scratch_shapes=[
            pltpu.VMEM((3, hidden_all, features), kind),
            pltpu.VMEM((3, shared_piece, features), kind),
            pltpu.VMEM((experts * row_count, features + LANES), kind),
            pltpu.VMEM((n, 2 * row_count, features), kind),
            pltpu.VMEM((n, row_count, features), kind),
            pltpu.VMEM((n, row_count, features), kind),
            pltpu.VMEM((n // 2, row_count, features), kind),
            pltpu.VMEM((n // 2 - 1, row_count, features), kind),
            DMA((4,)),
            DMA((n, 2)),
            DMA((n, 2)),
            DMA((n,)),
            DMA((n,)),
            DMA((3,)),
            DMA((3,)),
            DMA((n,)),
            DMA((n // 2,)),
            DMA((1,)),
            DMA((n,)),
            DMA((n,)),
            DMA((n,)),
            DMA((n,)),
            DMA((n,)),
            DMA((n // 2,)),
            DMA((n // 2,)),
            DMA((n // 2 - 1,)),
            DMA((n // 2 - 1,)),
            DMA((6,)),
        ],
        compiler_params=pltpu.CompilerParams(
            collective_id=0, has_side_effects=True, vmem_limit_bytes=60 * 1024 * 1024
        ),
    )(pieces, shared_stack, rows)


def body(*arguments):
    experts = lax.axis_size("fs") * lax.axis_size("tp")
    per_token = arguments[1].shape[1]
    pairs = lax.axis_size("gr") == 2 and lax.axis_size("tp") == 2
    if pairs and lax.axis_size("fs") % 2 == 0 and experts <= min(2 * per_token, LANES // 2):
        return direct_body(*arguments)
    return dispatch_body(*arguments)


def solution(mesh):
    in_specs = (
        P(("gr", "fs", "tp"), None),
        P(("gr", "fs", "tp"), None),
        P(("gr", "fs", "tp"), None),
        P(("gr", "tp")),
        P(None, "fs", ("gr", "tp")),
        P(None, "fs", ("gr", "tp")),
        P(None, "fs", ("gr", "tp")),
        P("fs", ("gr", "tp")),
        P("fs", ("gr", "tp")),
        P("fs", ("gr", "tp")),
    )
    out_specs = (
        P(("gr", "fs", "tp"), None),
        P(("fs", "tp"), None, None),
        P(("fs", "tp"), None, None),
        P(("fs", "tp"), None, None),
        P("fs", None),
        P("fs", None),
        P("fs", None),
    )
    return jax.shard_map(body, mesh=mesh, in_specs=in_specs, out_specs=out_specs, check_vma=False)
```

profile of v0, /device:TPU:10, one launch (start us, length us, event | category | flops | bytes accessed | tf_op | source)
XLA Modules:
  0.0 195.3 jit_solution(1399660088494963487)
XLA Ops:
  0.6 0.0 copy-start
  0.6 1.3 fusion
  1.9 0.7 select_reduce_fusion
  2.7 0.1 copy.25
  2.8 0.1 copy.24
  2.9 0.0 copy-start.3
  2.9 0.0 copy-start.7
  2.9 1.2 fusion.4
  4.1 0.7 pad_maximum_fusion.1.shared_ref
  4.8 0.0 copy-done
  4.8 0.2 fusion.1
  5.0 0.9 concatenate.3.rows_ref
  6.0 2.5 %fusion.2 = (bf16[16,1,48,512]{3,2,1,0:T(8,128)(2,1)S(1)}, bf16[16,1,48,512]{3,2,1,0:T(8,128)(2,1)S(1)}, bf16[16,1,48,512]{3,2,1,0:T(8,128)(2,1)S(1)}) fusion(f32[16,48,512]{2,1,0:T(8,128)S(1)} %copy-done.3, f32[512]{0:T(512)S(1)} %copy-done.7, f32[16,48,512]{2,1,0:T(8,128)} %param.15, f32[16,48,512]{2,1,0:T(8,128)} %param.16), kind=kLoop, calls=%fused_computation.7 | loop fusion | flops 1966080 | bytes 7079936 | tf_op jit(solution)/shard_map/stack | solution.py:518
  8.4 1.7 pad_maximum_fusion.pieces_ref
  10.1 175.3 %shard_map.153 = (bf16[128,2048]{1,0:T(8,128)(2,1)}, bf16[1,384,2048]{2,1,0:T(8,128)(2,1)}, bf16[1,384,2048]{2,1,0:T(8,128)(2,1)}, bf16[1,384,2048]{2,1,0:T(8,12...) custom-call(bf16[16,3,48,512]{3,2,1,0:T(8,128)(2,1)} %pad_maximum_fusion.pieces_ref, ...), custom_call_target="tpu_custom_call" | custom-call | tf_op jit(solution)/shard_map/pallas_call | solution.py:550
  185.4 1.9 copy.34
  187.3 2.8 %copy.35 = bf16[1,384,2048]{2,1,0:T(8,128)(2,1)} copy(bf16[1,384,2048]{2,1,0:T(8,128)(2,1)} %get-tuple-element.23) | data formatting | bytes 3145728
  190.1 1.1 copy.36
  191.3 0.8 copy-done.1
  192.1 1.1 copy.37
  193.2 0.7 copy.38
  193.9 0.0 copy-done.5
  193.9 0.7 copy.39
  194.6 0.7 copy.40
  (13 shorter events, 0.0 us)
Async XLA Ops:
  0.6 4.2 %copy-start = (bf16[128,2048]{1,0:T(8,128)(2,1)S(1)}, bf16[128,2048]{1,0:T(8,128)(2,1)}, u32[]{:S(2)}) copy-start(bf16[128,2048]{1,0:T(8,128)(2,1)} %param.10) | copy-start | bytes 1572868
  2.9 3.0 %copy-start.3 = (f32[16,48,512]{2,1,0:T(8,128)S(1)}, f32[16,48,512]{2,1,0:T(8,128)}, u32[]{:S(2)}) copy-start(f32[16,48,512]{2,1,0:T(8,128)} %param.14) | copy-start | bytes 4718596
  2.9 3.0 %copy-start.7 = (f32[512]{0:T(512)S(1)}, f32[512]{0:T(512)}, u32[]{:S(2)}) copy-start(f32[512]{0:T(512)} %param.13) | copy-start | bytes 6148
  187.3 2.9 %copy-start.2 = (bf16[1,384,2048]{2,1,0:T(8,128)(2,1)S(1)}, bf16[1,384,2048]{2,1,0:T(8,128)(2,1)}, u32[]{:S(2)}) copy-start(bf16[1,384,2048]{2,1,0:T(8,128)(2,1)} %get-tuple-element.24) | copy-start | bytes 4718596
  190.1 2.0 %copy-start.1 = (bf16[1,384,2048]{2,1,0:T(8,128)(2,1)S(1)}, bf16[1,384,2048]{2,1,0:T(8,128)(2,1)}, u32[]{:S(2)}) copy-start(bf16[1,384,2048]{2,1,0:T(8,128)(2,1)} %get-tuple-element.25) | copy-start | bytes 4718596
  192.1 1.2 copy-start.6
  192.1 1.9 copy-start.5
  192.1 2.6 %copy-start.4 = (bf16[64,2048]{1,0:T(8,128)(2,1)S(1)}, bf16[64,2048]{1,0:T(8,128)(2,1)}, u32[]{:S(2)}) copy-start(bf16[64,2048]{1,0:T(8,128)(2,1)} %get-tuple-element.28) | copy-start | bytes 786436
where the time goes:
time: 196 us; the launch traced here: 195 us
  Pallas kernels  175 us (89%)
  local copies, waits for them, and re-layouts  11.1 us (6%)
  other arithmetic  8.23 us (4%)
    pallas_call x1, Pallas kernels, direct_body(): pl.pallas_call(functools.partial(exchange_kernel, n), out_shape=(jax.Shap...  175 us
    unnamed x23, local copies, waits for them, and re-layouts  9.98 us
    another operation x2, other arithmetic, direct_body(): jnp.stack([gate_trained * gain_row, up_trained * gain_row, down_trained],...  4.12 us

commit v1 on v0

v1 whole, which is shorter than its diff:
```python
import functools

import jax
import jax.numpy as jnp
from jax import lax
from jax.experimental import pallas as pl
from jax.experimental.pallas import tpu as pltpu
from jax.sharding import PartitionSpec as P

epsilon = 1e-06
LANES = 128
MESH = pl.DeviceIdType.MESH


def contract_rows(inputs, matrix):
    return lax.dot_general(
        inputs, matrix, (((1,), (1,)), ((), ())), preferred_element_type=jnp.float32
    )


def swiglu_rows(inputs, gate_matrix, up_matrix, down_matrix):
    hidden = (
        jax.nn.silu(contract_rows(inputs, gate_matrix)) * contract_rows(inputs, up_matrix)
    ).astype(jnp.bfloat16)
    return jnp.dot(hidden, down_matrix, preferred_element_type=jnp.float32)


def dispatch_body(
    tokens,
    routes,
    route_weights,
    norm_gain,
    gate_trained,
    up_trained,
    down_trained,
    shared_gate_trained,
    shared_up_trained,
    shared_down_trained,
):
    gain_row = norm_gain[None, None, :]
    stacked = jnp.stack(
        [gate_trained * gain_row, up_trained * gain_row, down_trained], axis=1
    ).astype(jnp.bfloat16)
    halves = lax.all_to_all(
        lax.all_to_all(stacked[:, :, :, None, :], "fs", split_axis=0, concat_axis=2, tiled=True),
        "tp",
        split_axis=0,
        concat_axis=3,
        tiled=True,
    )
    owned = lax.all_gather(halves[:, :, :, None], "gr", axis=3, tiled=True)
    owned = owned.reshape(owned.shape[0], 3, owned.shape[2], -1)
    expert_gate = owned[:, 0]
    expert_up = owned[:, 1]
    expert_down = owned[:, 2]
    shared_gain = norm_gain[None, :]
    shared_stack = jnp.stack(
        [shared_gate_trained * shared_gain, shared_up_trained * shared_gain, shared_down_trained],
        axis=0,
    ).astype(jnp.bfloat16)
    shared_whole = lax.all_gather(shared_stack, ("gr", "tp"), axis=2, tiled=True)
    shared_gate = shared_whole[0]
    shared_up = shared_whole[1]
    shared_down = shared_whole[2]
    values = tokens.astype(jnp.float32)
    normed = (
        values * lax.rsqrt(jnp.mean(values * values, axis=1, keepdims=True) + epsilon)
    ).astype(jnp.bfloat16)
    row_count, features = normed.shape
    per_token = routes.shape[1]
    shared_out = swiglu_rows(
        normed,
        lax.all_gather(shared_gate, "fs", axis=0, tiled=True),
        lax.all_gather(shared_up, "fs", axis=0, tiled=True),
        lax.all_gather(shared_down, "fs", axis=0, tiled=True),
    )
    experts = lax.axis_size("fs") * lax.axis_size("tp")
    capacity = max(2, 3 * row_count * per_token // (2 * experts))
    chosen = routes.reshape(-1)
    onehot = (chosen[:, None] == jnp.arange(experts, dtype=jnp.int32)[None, :]).astype(jnp.int32)
    position = jnp.sum((jnp.cumsum(onehot, axis=0) - onehot) * onehot, axis=1)
    target = chosen * capacity + position
    source = (
        jnp.full((experts * capacity,), row_count, jnp.int32)
        .at[target]
        .set(jnp.arange(row_count * per_token, dtype=jnp.int32) // per_token)
    )
    padded = jnp.concatenate([normed, jnp.zeros((1, features), jnp.bfloat16)], axis=0)
    outgoing = padded[source].reshape(experts, capacity, features)
    arrived = lax.all_to_all(outgoing, ("fs", "tp"), split_axis=0, concat_axis=0, tiled=True)
    item_count = arrived.shape[1]
    result = swiglu_rows(
        arrived.reshape(-1, features), expert_gate[0], expert_up[0], expert_down[0]
    )
    result = result.astype(jnp.bfloat16).reshape(experts, item_count, features)
    returned = lax.all_to_all(result, ("fs", "tp"), split_axis=0, concat_axis=0, tiled=True)
    picked = returned.reshape(experts * capacity, features)[target].astype(jnp.float32)
    picked = picked.reshape(row_count, per_token, features)
    routed = jnp.sum(picked * route_weights[:, :, None], axis=1)
    combined = (routed + shared_out).astype(jnp.bfloat16)
    return (combined, expert_gate, expert_up, expert_down, shared_gate, shared_up, shared_down)


def exchange_kernel(
    n,
    pieces_ref,
    shared_ref,
    rows_ref,
    combined_ref,
    gate_ref,
    up_ref,
    down_ref,
    shared_gate_ref,
    shared_up_ref,
    shared_down_ref,
    weights,
    owned,
    shared,
    rows,
    select,
    parts,
    pair_in,
    sums,
    side_in,
    sums_in,
    local_sem,
    slice_out_sem,
    slice_sem,
    piece_sem,
    weight_sem,
    column_out_sem,
    column_sem,
    shared_out_sem,
    shared_sem,
    row_out_sem,
    row_side_sem,
    row_back_sem,
    row_sem,
    row_pair_out_sem,
    row_pair_sem,
    part_sem,
    part_recv_sem,
    side_sem,
    side_recv_sem,
    sum_sem,
    sum_recv_sem,
    out_sem,
):
    gr, fs, tp = lax.axis_index("gr"), lax.axis_index("fs"), lax.axis_index("tp")
    other = 1 - tp
    across = (1 - gr, fs, tp)
    across_twin = (1 - gr, fs, other)
    twin = (gr, fs, other)
    expert = fs * 2 + tp
    width = pieces_ref.shape[2]
    hidden_piece = pieces_ref.shape[1] // (2 * n)
    hidden = n * hidden_piece
    shared_piece = shared_ref.shape[1]
    extra = shared_piece // 2
    features = 4 * width
    row_count = rows_ref.shape[0]
    depth = n // 2
    outer, inner = lax.div(fs, 2), lax.rem(fs, 2)
    beside = (gr, outer * 2 + 1 - inner, tp)
    toward = jnp.where(outer < depth // 2, 1, -1)

    barrier = pltpu.get_barrier_semaphore()
    for device in (across, across_twin, twin):
        pl.semaphore_signal(barrier, inc=1, device_id=device, device_id_type=MESH)
    for k in range(1, n):
        for t in range(2):
            pl.semaphore_signal(
                barrier, inc=1, device_id=(gr, lax.rem(fs + k, n), t), device_id_type=MESH
            )
    pl.semaphore_wait(barrier, 2 * n + 1)

    def remote(src, dst, send, recv, device):
        return pltpu.make_async_remote_copy(
            src_ref=src,
            dst_ref=dst,
            send_sem=send,
            recv_sem=recv,
            device_id=device,
            device_id_type=MESH,
        )

    def columns(g, t):
        return pl.ds(pl.multiple_of((g * 2 + t) * width, width), width)

    def piece(e):
        return pieces_ref.at[:, pl.ds(pl.multiple_of(e * hidden_piece, 16), hidden_piece), :]

    def portion(t):
        return pieces_ref.at[:, pl.ds(pl.multiple_of(t * hidden, 16), hidden), :]

    def sliced(g, t):
        return weights.at[:, pl.ds(0, hidden), columns(g, t)]

    def slab(source, span):
        start = pl.multiple_of(source * hidden_piece, 16)
        return owned.at[:, pl.ds(start, hidden_piece), span]

    def row_block(source, t):
        start = pl.multiple_of((source * 2 + t) * row_count, row_count)
        return rows.at[pl.ds(start, row_count)]

    def nearby(k):
        place = lax.rem(outer + toward * lax.div(k, 2) + depth, depth)
        return place * 2 + jnp.where(lax.rem(k, 2) == 0, inner, 1 - inner)

    half = pl.ds(pl.multiple_of(gr * 2 * width, width), 2 * width)
    far_half = pl.ds(pl.multiple_of((1 - gr) * 2 * width, width), 2 * width)

    def slice_send(index, t, device):
        return remote(
            portion(t), sliced(gr, tp), slice_out_sem.at[index], slice_sem.at[index], device
        )

    def piece_send(d, t):
        return remote(
            piece(d * 2 + t),
            slab(fs, columns(gr, tp)),
            piece_sem.at[d, t],
            weight_sem.at[fs, tp],
            (gr, d, t),
        )

    def column_send(source):
        return remote(
            slab(source, half),
            slab(source, half),
            column_out_sem.at[source],
            column_sem.at[source],
            across,
        )

    def row_own(send, recv, device):
        return remote(rows_ref, row_block(fs, tp), send, recv, device)

    def row_move(source, send, recv, device):
        return remote(row_block(source, tp), row_block(source, tp), send, recv, device)

    def row_onward(source, step):
        return row_move(
            source,
            row_out_sem.at[source],
            row_sem.at[source],
            (gr, (outer + step) * 2 + inner, tp),
        )

    def row_beside(source):
        return row_move(source, row_side_sem.at[lax.div(source, 2)], row_sem.at[source], beside)

    def row_relay(source):
        return row_move(source, row_pair_out_sem.at[source], row_pair_sem.at[source], twin)

    own_up = row_own(row_out_sem.at[fs], row_sem.at[fs], (gr, (outer + 1) * 2 + inner, tp))
    own_back = row_own(row_back_sem.at[0], row_sem.at[fs], (gr, (outer - 1) * 2 + inner, tp))
    own_beside = row_own(row_side_sem.at[outer], row_sem.at[fs], beside)
    own_relay = row_own(row_pair_out_sem.at[fs], row_pair_sem.at[fs], twin)

    def at_distance(distance, action):
        for step in (1, -1):
            place = outer - step * distance

            @pl.when((place >= 0) & (place < depth))
            def _():
                action(place, step)

    def onward_exists(step):
        return (outer + step >= 0) & (outer + step < depth)

    @pl.when(outer < depth - 1)
    def _():
        own_up.start()

    @pl.when(outer > 0)
    def _():
        own_back.start()

    own_beside.start()
    shared_far = remote(
        shared_ref, shared.at[:, :, columns(gr, tp)], shared_out_sem.at[0], shared_sem.at[0], across
    )
    shared_far.start()
    slice_far = slice_send(0, tp, across)
    slice_cross = slice_send(1, other, across_twin)
    slice_twin = slice_send(2, other, twin)
    slice_far.start()
    slice_cross.start()
    own_relay.start()
    slice_twin.start()
    shared_twin = remote(
        shared_ref, shared.at[:, :, columns(gr, tp)], shared_out_sem.at[1], shared_sem.at[1], twin
    )
    shared_twin.start()
    twin_piece = piece_send(fs, other)
    twin_piece.start()

    def ship(step, distances):
        for distance in distances:
            place = outer + step * distance

            @pl.when((place >= 0) & (place < depth))
            def _():
                piece_send(place * 2 + inner, 0).start()
                piece_send(place * 2 + inner, 1).start()

    @pl.when(outer == 0)
    def _():
        ship(1, (1,))

    @pl.when(outer == depth - 1)
    def _():
        ship(-1, (1,))

    own_rows = pltpu.make_async_copy(rows_ref, row_block(fs, tp), local_sem.at[0])
    own_slice = pltpu.make_async_copy(portion(tp), sliced(gr, tp), local_sem.at[1])
    own_piece = pltpu.make_async_copy(piece(expert), slab(fs, columns(gr, tp)), local_sem.at[2])
    own_shared = pltpu.make_async_copy(
        shared_ref, shared.at[:, :, columns(gr, tp)], local_sem.at[3]
    )
    locals_ = (own_rows, own_slice, own_piece, own_shared)
    for copy in locals_:
        copy.start()
    lane = lax.broadcasted_iota(jnp.int32, select.shape, 0)
    unit = lax.broadcasted_iota(jnp.int32, select.shape, 1)
    first = (jnp.where(lane < LANES // 2, lane, lane - LANES // 2) - tp * n) * hidden_piece
    inside = (unit >= first) & (unit < first + hidden_piece) & (unit < hidden)
    select[...] = jnp.where(inside, 1.0, 0.0).astype(select.dtype)

    def take_rows(source):
        row_move(source, row_out_sem.at[source], row_sem.at[source], twin).wait_recv()

    def arrive(place, step):
        source = place * 2 + inner
        take_rows(source)

        @pl.when(onward_exists(step))
        def _():
            row_onward(source, step).start()

        row_beside(source).start()
        row_relay(source).start()

        @pl.when(place == (0 if step == 1 else depth - 1))
        def _():
            ship(step, range(1, depth))

    def arrive_beside(place, step):
        source = place * 2 + 1 - inner
        take_rows(source)
        row_relay(source).start()

    at_distance(1, arrive)
    for copy in locals_:
        copy.wait()
    far_columns = shared.at[:, :, columns(1 - gr, tp)]
    remote(shared_ref, far_columns, shared_out_sem.at[0], shared_sem.at[0], across).wait_recv()
    shared_relay = remote(far_columns, far_columns, shared_out_sem.at[2], shared_sem.at[2], twin)
    shared_relay.start()
    arrive_beside(outer, 0)
    for distance in range(2, depth):
        at_distance(distance, arrive)
        if distance == 2:

            @pl.when(outer == 0)
            def _():
                ship(1, range(2, depth))

            @pl.when(outer == depth - 1)
            def _():
                ship(-1, range(2, depth))

        at_distance(distance - 1, arrive_beside)

    for k in range(1, n, 2):
        d = nearby(k)
        piece_send(d, 0).start()
        piece_send(d, 1).start()

    def take_twin_piece(source, t):
        remote(
            piece(0),
            slab(source, columns(gr, t)),
            piece_sem.at[fs, other],
            weight_sem.at[source, t],
            twin,
        ).wait_recv()

    take_twin_piece(fs, other)
    column_send(fs).start()

    remote(
        shared_ref, shared.at[:, :, columns(gr, other)], shared_out_sem.at[1], shared_sem.at[1], twin
    ).wait_recv()
    last_columns = shared.at[:, :, columns(1 - gr, other)]
    remote(shared_ref, last_columns, shared_out_sem.at[2], shared_sem.at[2], twin).wait_recv()
    outs = []
    for j, ref in enumerate((shared_gate_ref, shared_up_ref, shared_down_ref)):
        outs.append(pltpu.make_async_copy(shared.at[j], ref, out_sem.at[3 + j]))
    for copy in outs:
        copy.start()
    tail = pltpu.make_async_copy(
        shared.at[:, pl.ds(pl.multiple_of(tp * extra, extra), extra), :],
        weights.at[:, pl.ds(hidden, extra), :],
        local_sem.at[4],
    )
    tail.start()
    tail.wait()
    remote(portion(tp), sliced(gr, other), slice_out_sem.at[2], slice_sem.at[2], twin).wait_recv()
    remote(portion(tp), sliced(1 - gr, tp), slice_out_sem.at[0], slice_sem.at[0], across).wait_recv()
    remote(
        portion(tp), sliced(1 - gr, other), slice_out_sem.at[1], slice_sem.at[1], across
    ).wait_recv()

    def part_send(k):
        return remote(
            parts.at[k, pl.ds(pl.multiple_of(other * row_count, row_count), row_count), :],
            pair_in.at[k],
            part_sem.at[k],
            part_recv_sem.at[k],
            twin,
        )

    def place_of(j):
        return lax.rem(outer + toward * (j + 1) + depth, depth)

    def side_send(j):
        return remote(
            sums.at[2 * j], side_in.at[j], side_sem.at[j], side_recv_sem.at[j], beside
        )

    def sum_send(j):
        place = place_of(j)
        slot = lax.rem(outer - place + 2 * depth - 1, depth)
        return remote(
            sums.at[2 * j + 1],
            sums_in.at[slot],
            sum_sem.at[j],
            sum_recv_sem.at[slot],
            (gr, place * 2 + inner, tp),
        )

    chunk = 32

    def add_pair(k):
        part_send(k).wait_recv()

        @pl.loop(0, row_count // chunk)
        def _(i):
            at = pl.multiple_of(i * chunk, chunk)
            mine = pl.multiple_of(tp * row_count + i * chunk, chunk)
            value = parts[k, pl.ds(mine, chunk), :].astype(jnp.float32)
            value = value + pair_in[k, pl.ds(at, chunk), :].astype(jnp.float32)
            sums[k, pl.ds(at, chunk), :] = value.astype(jnp.bfloat16)

    def add_both(j):
        k = 2 * j + 1
        part_send(k).wait_recv()
        side_send(j).wait_recv()

        @pl.loop(0, row_count // chunk)
        def _(i):
            at = pl.multiple_of(i * chunk, chunk)
            mine = pl.multiple_of(tp * row_count + i * chunk, chunk)
            value = parts[k, pl.ds(mine, chunk), :].astype(jnp.float32)
            value = value + pair_in[k, pl.ds(at, chunk), :].astype(jnp.float32)
            value = value + side_in[j, pl.ds(at, chunk), :].astype(jnp.float32)
            sums[k, pl.ds(at, chunk), :] = value.astype(jnp.bfloat16)

    def take_weights(source):
        take_twin_piece(source, 0)
        take_twin_piece(source, 1)
        column_send(source).start()

    @pl.loop(0, n)
    def _(k):
        j = lax.div(k, 2)
        d = place_of(j) * 2 + jnp.where(lax.rem(k, 2) == 0, 1 - inner, inner)

        @pl.when(k == n - 4)
        def _():
            at_distance(depth - 1, arrive_beside)

        remote(
            row_block(d, other), row_block(d, other), row_pair_out_sem.at[d], row_pair_sem.at[d], twin
        ).wait_recv()
        block = pl.ds(pl.multiple_of(d * 2 * row_count, 2 * row_count), 2 * row_count)
        inputs = rows[block, 0:features]
        scale = jnp.dot(
            rows[block, features : features + LANES],
            select[...],
            preferred_element_type=jnp.float32,
        )
        gate = contract_rows(inputs, weights[0])
        up = contract_rows(inputs, weights[1])
        position = lax.broadcasted_iota(jnp.int32, gate.shape, 1)
        scale = jnp.where(position < hidden, scale, 1.0)
        units = (gate / (1.0 + jnp.exp(-gate)) * up * scale).astype(jnp.bfloat16)
        for c in range(4):
            span = pl.ds(c * width, width)
            parts[k, :, span] = jnp.dot(
                units, weights[2, :, span], preferred_element_type=jnp.float32
            ).astype(jnp.bfloat16)
        part_send(k).start()

        @pl.when(lax.rem(k, 2) == 1)
        def _():
            add_pair(k - 1)
            side_send(j).start()

        @pl.when((k > 0) & (k < depth))
        def _():
            take_weights(nearby(2 * k))

    take_weights(nearby(1))
    for j in range(depth - 1):
        take_weights(nearby(2 * j + 3))
        add_both(j)
        sum_send(j).start()

    for k in range(n):
        source = nearby(k)
        remote(
            slab(source, far_half),
            slab(source, far_half),
            column_out_sem.at[source],
            column_sem.at[source],
            across,
        ).wait_recv()
    for j, ref in enumerate((gate_ref, up_ref, down_ref)):
        copy = pltpu.make_async_copy(owned.at[j], ref.at[0], out_sem.at[j])
        copy.start()
        outs.append(copy)

    add_both(depth - 1)
    for j in range(depth - 1):
        remote(sums.at[0], sums_in.at[j], sum_sem.at[j], sum_recv_sem.at[j], twin).wait_recv()

    @pl.loop(0, row_count // chunk)
    def _(i):
        at = pl.ds(pl.multiple_of(i * chunk, chunk), chunk)
        total = sums[n - 1, at, :].astype(jnp.float32)
        for j in range(depth - 1):
            total = total + sums_in[j, at, :].astype(jnp.float32)
        combined_ref[at, :] = total.astype(jnp.bfloat16)

    @pl.when(outer < depth - 1)
    def _():
        own_up.wait_send()

    @pl.when(outer > 0)
    def _():
        own_back.wait_send()

    for copy in (
        own_beside,
        own_relay,
        shared_far,
        slice_far,
        slice_cross,
        slice_twin,
        shared_twin,
        twin_piece,
        shared_relay,
    ):
        copy.wait_send()

    def sent(place, step):
        source = place * 2 + inner

        @pl.when(onward_exists(step))
        def _():
            row_onward(source, step).wait_send()

        row_beside(source).wait_send()

    for distance in range(1, depth):
        at_distance(distance, sent)
    column_send(fs).wait_send()
    for k in range(1, n):
        d = lax.rem(fs + k, n)
        piece_send(d, 0).wait_send()
        piece_send(d, 1).wait_send()
        column_send(d).wait_send()
        row_relay(d).wait_send()
    for k in range(n):
        part_send(k).wait_send()
    for j in range(depth):
        side_send(j).wait_send()
    for j in range(depth - 1):
        sum_send(j).wait_send()
    for copy in outs:
        copy.wait()


def direct_body(
    tokens,
    routes,
    route_weights,
    norm_gain,
    gate_trained,
    up_trained,
    down_trained,
    shared_gate_trained,
    shared_up_trained,
    shared_down_trained,
):
    gain_row = norm_gain[None, None, :]
    experts, hidden_piece, width = gate_trained.shape
    pieces = (
        jnp.stack([gate_trained * gain_row, up_trained * gain_row, down_trained], axis=0)
        .astype(jnp.bfloat16)
        .reshape(3, experts * hidden_piece, width)
    )
    shared_gain = norm_gain[None, :]
    shared_stack = jnp.stack(
        [shared_gate_trained * shared_gain, shared_up_trained * shared_gain, shared_down_trained],
        axis=0,
    ).astype(jnp.bfloat16)
    values = tokens.astype(jnp.float32)
    normed = (
        values * lax.rsqrt(jnp.mean(values * values, axis=1, keepdims=True) + epsilon)
    ).astype(jnp.bfloat16)
    n = lax.axis_size("fs")
    row_count, features = normed.shape
    shared_piece = shared_stack.shape[1]
    numbers = jnp.arange(LANES // 2, dtype=jnp.int32)
    factors = jnp.sum(
        jnp.where(routes[:, :, None] == numbers, route_weights[:, :, None], 0.0), axis=1
    )
    high = lax.reduce_precision(factors, 8, 7)
    rows = jnp.concatenate(
        [normed, high.astype(jnp.bfloat16), (factors - high).astype(jnp.bfloat16)], axis=1
    )
    hidden = n * hidden_piece
    hidden_all = hidden + shared_piece // 2
    vmem = pl.BlockSpec(memory_space=pltpu.VMEM)
    hbm = pl.BlockSpec(memory_space=pl.ANY)
    kind = jnp.bfloat16
    expert_shape = jax.ShapeDtypeStruct((1, hidden, features), kind)
    shared_shape = jax.ShapeDtypeStruct((shared_piece, features), kind)
    DMA = pltpu.SemaphoreType.DMA
    return pl.pallas_call(
        functools.partial(exchange_kernel, n),
        out_shape=(jax.ShapeDtypeStruct((row_count, features), kind),)
        + (expert_shape,) * 3
        + (shared_shape,) * 3,
        in_specs=[vmem] * 3,
        out_specs=(vmem,) + (hbm,) * 6,
        scratch_shapes=[
            pltpu.VMEM((3, hidden_all, features), kind),
            pltpu.VMEM((3, hidden, features), kind),
            pltpu.VMEM((3, shared_piece, features), kind),
            pltpu.VMEM((experts * row_count, features + LANES), kind),
            pltpu.VMEM((LANES, hidden_all), kind),
            pltpu.VMEM((n, 2 * row_count, features), kind),
            pltpu.VMEM((n, row_count, features), kind),
            pltpu.VMEM((n, row_count, features), kind),
            pltpu.VMEM((n // 2, row_count, features), kind),
            pltpu.VMEM((n // 2 - 1, row_count, features), kind),
            DMA((5,)),
            DMA((3,)),
            DMA((3,)),
            DMA((n, 2)),
            DMA((n, 2)),
            DMA((n,)),
            DMA((n,)),
            DMA((3,)),
            DMA((3,)),
            DMA((n,)),
            DMA((n // 2,)),
            DMA((1,)),
            DMA((n,)),
            DMA((n,)),
            DMA((n,)),
            DMA((n,)),
            DMA((n,)),
            DMA((n // 2,)),
            DMA((n // 2,)),
            DMA((n // 2 - 1,)),
            DMA((n // 2 - 1,)),
            DMA((6,)),
        ],
        compiler_params=pltpu.CompilerParams(
            collective_id=0, has_side_effects=True, vmem_limit_bytes=60 * 1024 * 1024
        ),
    )(pieces, shared_stack, rows)


def body(*arguments):
    experts = lax.axis_size("fs") * lax.axis_size("tp")
    per_token = arguments[1].shape[1]
    pairs = lax.axis_size("gr") == 2 and lax.axis_size("tp") == 2
    if pairs and lax.axis_size("fs") % 2 == 0 and experts <= min(2 * per_token, LANES // 2):
        return direct_body(*arguments)
    return dispatch_body(*arguments)


def solution(mesh):
    in_specs = (
        P(("gr", "fs", "tp"), None),
        P(("gr", "fs", "tp"), None),
        P(("gr", "fs", "tp"), None),
        P(("gr", "tp")),
        P(None, "fs", ("gr", "tp")),
        P(None, "fs", ("gr", "tp")),
        P(None, "fs", ("gr", "tp")),
        P("fs", ("gr", "tp")),
        P("fs", ("gr", "tp")),
        P("fs", ("gr", "tp")),
    )
    out_specs = (
        P(("gr", "fs", "tp"), None),
        P(("fs", "tp"), None, None),
        P(("fs", "tp"), None, None),
        P(("fs", "tp"), None, None),
        P("fs", None),
        P("fs", None),
        P("fs", None),
    )
    return jax.shard_map(body, mesh=mesh, in_specs=in_specs, out_specs=out_specs, check_vma=False)
```

time: 196 us -> 167 us (0.85)
  the two profiles are of different devices: /device:TPU:10 before, /device:TPU:0 now
where the time goes in v1:
time: 167 us
  Pallas kernels  146 us (87%)
  local copies, waits for them, and re-layouts  12.4 us (7%)
  other arithmetic  7.75 us (5%)
    pallas_call x1, Pallas kernels, direct_body(): pl.pallas_call(functools.partial(exchange_kernel, n), out_shape=(jax.Shap...  146 us
    unnamed x25, local copies, waits for them, and re-layouts  11.3 us

profile of v1, /device:TPU:0, one launch (start us, length us, event | category | flops | bytes accessed | tf_op | source)
XLA Modules:
  0.0 166.8 jit_solution(9580178732569981934)
XLA Ops:
  0.6 0.0 copy-start
  0.6 1.3 fusion
  1.9 0.7 select_reduce_fusion
  2.7 0.1 copy.22
  2.8 0.1 copy.21
  2.9 0.0 copy-start.1
  2.9 1.2 fusion.2
  4.1 0.7 pad_maximum_fusion.1.shared_ref
  4.8 0.2 fusion.1
  5.0 0.0 copy-start.8
  5.0 0.9 concatenate.5.rows_ref
  6.0 0.1 convert.26
  6.1 1.3 copy-done.4
  7.4 1.9 %multiply_convert_fusion.1 = (bf16[16,48,512]{2,1,0:T(8,128)(2,1)S(1)}, bf16[16,48,512]{2,1,0:T(8,128)(2,1)S(1)}) fusion(f32[16,48,512]{2,1,0:T(8,128)S(1)} %copy-done.4, f32[512]{0:T(512)S(1)} %copy-done.8, f32[16,48,512]{2,1,0:T(8,128)} %param.15), kind=kLoop, calls=%fused_computation.2 | loop fusion | flops 1572864 | bytes 4720640 | tf_op jit(solution)/shard_map/convert.11
  9.2 1.7 pad_maximum_fusion.pieces_ref
  10.9 145.9 %shard_map.153 = (bf16[128,2048]{1,0:T(8,128)(2,1)}, bf16[1,384,2048]{2,1,0:T(8,128)(2,1)}, bf16[1,384,2048]{2,1,0:T(8,128)(2,1)}, bf16[1,384,2048]{2,1,0:T(8,12...) custom-call(bf16[3,768,512]{2,1,0:T(8,128)(2,1)} %pad_maximum_fusion.pieces_ref, ...), custom_call_target="tpu_custom_call" | custom-call | tf_op jit(solution)/shard_map/pallas_call | solution.py:645
  156.8 1.9 %copy.31 = bf16[128,2048]{1,0:T(8,128)(2,1)} copy(bf16[128,2048]{1,0:T(8,128)(2,1)} %get-tuple-element.21) | data formatting | bytes 1048576
  158.7 2.8 %copy.32 = bf16[1,384,2048]{2,1,0:T(8,128)(2,1)} copy(bf16[1,384,2048]{2,1,0:T(8,128)(2,1)} %get-tuple-element.22) | data formatting | bytes 3145728
  161.5 1.1 copy.33
  162.7 0.8 copy-done.2
  163.5 1.1 copy.34
  164.7 0.7 copy.35
  165.4 0.7 copy.36
  166.1 0.7 copy.37
  (16 shorter events, 0.1 us)
Async XLA Ops:
  0.6 4.2 %copy-start = (bf16[128,2048]{1,0:T(8,128)(2,1)S(1)}, bf16[128,2048]{1,0:T(8,128)(2,1)}, u32[]{:S(2)}) copy-start(bf16[128,2048]{1,0:T(8,128)(2,1)} %param.10) | copy-start | bytes 1572868
  2.9 3.0 %copy-start.1 = (f32[16,48,512]{2,1,0:T(8,128)S(1)}, f32[16,48,512]{2,1,0:T(8,128)}, u32[]{:S(2)}) copy-start(f32[16,48,512]{2,1,0:T(8,128)} %param.16) | copy-start | bytes 4718596
  5.0 1.1 copy-start.8
  6.0 1.4 copy-start.4
  158.7 2.9 %copy-start.3 = (bf16[1,384,2048]{2,1,0:T(8,128)(2,1)S(1)}, bf16[1,384,2048]{2,1,0:T(8,128)(2,1)}, u32[]{:S(2)}) copy-start(bf16[1,384,2048]{2,1,0:T(8,128)(2,1)} %get-tuple-element.23) | copy-start | bytes 4718596
  161.5 2.0 %copy-start.2 = (bf16[1,384,2048]{2,1,0:T(8,128)(2,1)S(1)}, bf16[1,384,2048]{2,1,0:T(8,128)(2,1)}, u32[]{:S(2)}) copy-start(bf16[1,384,2048]{2,1,0:T(8,128)(2,1)} %get-tuple-element.24) | copy-start | bytes 4718596
  163.5 1.2 copy-start.7
  163.5 1.9 %copy-start.6 = (bf16[64,2048]{1,0:T(8,128)(2,1)S(1)}, bf16[64,2048]{1,0:T(8,128)(2,1)}, u32[]{:S(2)}) copy-start(bf16[64,2048]{1,0:T(8,128)(2,1)} %get-tuple-element.26) | copy-start | bytes 786436
  163.5 2.6 %copy-start.5 = (bf16[64,2048]{1,0:T(8,128)(2,1)S(1)}, bf16[64,2048]{1,0:T(8,128)(2,1)}, u32[]{:S(2)}) copy-start(bf16[64,2048]{1,0:T(8,128)(2,1)} %get-tuple-element.27) | copy-start | bytes 786436

commit v2 on v1

--- a/solution.py
+++ b/solution.py
@@ -103,21 +103,30 @@
 
 def exchange_kernel(
     n,
-    pieces_ref,
-    shared_ref,
-    rows_ref,
+    tokens_hbm,
+    routes_hbm,
+    route_weights_hbm,
+    gain_hbm,
+    gate_hbm,
+    up_hbm,
+    down_hbm,
+    shared_gate_hbm,
+    shared_up_hbm,
+    shared_down_hbm,
     combined_ref,
-    gate_ref,
-    up_ref,
-    down_ref,
-    shared_gate_ref,
-    shared_up_ref,
-    shared_down_ref,
-    weights,
     owned,
     shared,
+    weights,
     rows,
     select,
+    tokens_ref,
+    routes_ref,
+    route_weights_ref,
+    gain_ref,
+    shared_stage,
+    stage,
+    pieces,
+    shared_mine,
     parts,
     pair_in,
     sums,
@@ -144,7 +153,8 @@
     side_recv_sem,
     sum_sem,
     sum_recv_sem,
-    out_sem,
+    stage_sem,
+    input_sem,
 ):
     gr, fs, tp = lax.axis_index("gr"), lax.axis_index("fs"), lax.axis_index("tp")
     other = 1 - tp
@@ -152,17 +162,38 @@
     across_twin = (1 - gr, fs, other)
     twin = (gr, fs, other)
     expert = fs * 2 + tp
-    width = pieces_ref.shape[2]
-    hidden_piece = pieces_ref.shape[1] // (2 * n)
+    width = pieces.shape[2]
+    hidden_piece = pieces.shape[1] // (2 * n)
     hidden = n * hidden_piece
-    shared_piece = shared_ref.shape[1]
+    shared_piece = shared_mine.shape[1]
     extra = shared_piece // 2
     features = 4 * width
-    row_count = rows_ref.shape[0]
+    row_count = tokens_ref.shape[0]
     depth = n // 2
     outer, inner = lax.div(fs, 2), lax.rem(fs, 2)
     beside = (gr, outer * 2 + 1 - inner, tp)
     toward = jnp.where(outer < depth // 2, 1, -1)
+
+    inputs_in = []
+    for i, (source, target) in enumerate(
+        (
+            (tokens_hbm, tokens_ref),
+            (routes_hbm, routes_ref),
+            (route_weights_hbm, route_weights_ref),
+            (gain_hbm, gain_ref),
+            (shared_gate_hbm, shared_stage.at[0]),
+            (shared_up_hbm, shared_stage.at[1]),
+            (shared_down_hbm, shared_stage.at[2]),
+        )
+    ):
+        inputs_in.append(pltpu.make_async_copy(source, target, input_sem.at[i]))
+        inputs_in[i].start()
+    staged = {}
+    for t in (0, 1):
+        for j, ref in enumerate((gate_hbm, up_hbm, down_hbm)):
+            part = pl.ds(t * hidden, hidden)
+            staged[j, t] = pltpu.make_async_copy(ref.at[part], stage.at[j, part], stage_sem.at[j, t])
+            staged[j, t].start()
 
     barrier = pltpu.get_barrier_semaphore()
     for device in (across, across_twin, twin):
@@ -172,6 +203,48 @@
             pl.semaphore_signal(
                 barrier, inc=1, device_id=(gr, lax.rem(fs + k, n), t), device_id_type=MESH
             )
+
+    own_start = pl.multiple_of(expert * row_count, row_count)
+    few = 16
+    for copy in inputs_in:
+        copy.wait()
+
+    @pl.loop(0, row_count // few)
+    def _(i):
+        at = pl.multiple_of(i * few, few)
+        values = tokens_ref[pl.ds(at, few), :].astype(jnp.float32)
+        mean = jnp.mean(values * values, axis=1, keepdims=True)
+        normed = (values * lax.rsqrt(mean + epsilon)).astype(jnp.bfloat16)
+        rows[pl.ds(own_start + at, few), 0:features] = normed
+
+    number = lax.broadcasted_iota(jnp.int32, (LANES // 2, row_count), 0)
+    factors = jnp.zeros(number.shape, jnp.float32)
+    for k in range(routes_ref.shape[0]):
+        named = routes_ref[k : k + 1, :] == number
+        factors = factors + jnp.where(named, route_weights_ref[k : k + 1, :], 0.0)
+    high = factors.astype(jnp.bfloat16).astype(jnp.float32)
+    both = jnp.concatenate([high, factors - high], axis=0)
+    rows[pl.ds(own_start, row_count), features : features + LANES] = both.T.astype(jnp.bfloat16)
+
+    gain = gain_ref[...]
+    for j in range(3):
+        value = shared_stage[j] if j == 2 else shared_stage[j] * gain
+        shared_mine[j] = value.astype(jnp.bfloat16)
+    for t in (0, 1):
+        for j in range(3):
+            staged[j, t].wait()
+
+            @pl.loop(0, n)
+            def _(i):
+                at = pl.ds(pl.multiple_of((t * n + i) * hidden_piece, hidden_piece), hidden_piece)
+                value = stage[j, at, :] if j == 2 else stage[j, at, :] * gain_ref[...]
+                pieces[j, at, :] = value.astype(jnp.bfloat16)
+
+    lane = lax.broadcasted_iota(jnp.int32, select.shape, 0)
+    unit = lax.broadcasted_iota(jnp.int32, select.shape, 1)
+    first = (jnp.where(lane < LANES // 2, lane, lane - LANES // 2) - tp * n) * hidden_piece
+    inside = (unit >= first) & (unit < first + hidden_piece) & (unit < hidden)
+    select[...] = jnp.where(inside, 1.0, 0.0).astype(select.dtype)
     pl.semaphore_wait(barrier, 2 * n + 1)
 
     def remote(src, dst, send, recv, device):
@@ -188,10 +261,10 @@
         return pl.ds(pl.multiple_of((g * 2 + t) * width, width), width)
 
     def piece(e):
-        return pieces_ref.at[:, pl.ds(pl.multiple_of(e * hidden_piece, 16), hidden_piece), :]
+        return pieces.at[:, pl.ds(pl.multiple_of(e * hidden_piece, 16), hidden_piece), :]
 
     def portion(t):
-        return pieces_ref.at[:, pl.ds(pl.multiple_of(t * hidden, 16), hidden), :]
+        return pieces.at[:, pl.ds(pl.multiple_of(t * hidden, 16), hidden), :]
 
     def sliced(g, t):
         return weights.at[:, pl.ds(0, hidden), columns(g, t)]
@@ -234,9 +307,6 @@
             across,
         )
 
-    def row_own(send, recv, device):
-        return remote(rows_ref, row_block(fs, tp), send, recv, device)
-
     def row_move(source, send, recv, device):
         return remote(row_block(source, tp), row_block(source, tp), send, recv, device)
 
@@ -254,10 +324,10 @@
     def row_relay(source):
         return row_move(source, row_pair_out_sem.at[source], row_pair_sem.at[source], twin)
 
-    own_up = row_own(row_out_sem.at[fs], row_sem.at[fs], (gr, (outer + 1) * 2 + inner, tp))
-    own_back = row_own(row_back_sem.at[0], row_sem.at[fs], (gr, (outer - 1) * 2 + inner, tp))
-    own_beside = row_own(row_side_sem.at[outer], row_sem.at[fs], beside)
-    own_relay = row_own(row_pair_out_sem.at[fs], row_pair_sem.at[fs], twin)
+    own_up = row_move(fs, row_out_sem.at[fs], row_sem.at[fs], (gr, (outer + 1) * 2 + inner, tp))
+    own_back = row_move(fs, row_back_sem.at[0], row_sem.at[fs], (gr, (outer - 1) * 2 + inner, tp))
+    own_beside = row_move(fs, row_side_sem.at[outer], row_sem.at[fs], beside)
+    own_relay = row_move(fs, row_pair_out_sem.at[fs], row_pair_sem.at[fs], twin)
 
     def at_distance(distance, action):
         for step in (1, -1):
@@ -280,7 +350,7 @@
 
     own_beside.start()
     shared_far = remote(
-        shared_ref, shared.at[:, :, columns(gr, tp)], shared_out_sem.at[0], shared_sem.at[0], across
+        shared_mine, shared.at[:, :, columns(gr, tp)], shared_out_sem.at[0], shared_sem.at[0], across
     )
     shared_far.start()
     slice_far = slice_send(0, tp, across)
@@ -291,7 +361,7 @@
     own_relay.start()
     slice_twin.start()
     shared_twin = remote(
-        shared_ref, shared.at[:, :, columns(gr, tp)], shared_out_sem.at[1], shared_sem.at[1], twin
+        shared_mine, shared.at[:, :, columns(gr, tp)], shared_out_sem.at[1], shared_sem.at[1], twin
     )
     shared_twin.start()
     twin_piece = piece_send(fs, other)
@@ -314,20 +384,14 @@
     def _():
         ship(-1, (1,))
 
-    own_rows = pltpu.make_async_copy(rows_ref, row_block(fs, tp), local_sem.at[0])
     own_slice = pltpu.make_async_copy(portion(tp), sliced(gr, tp), local_sem.at[1])
     own_piece = pltpu.make_async_copy(piece(expert), slab(fs, columns(gr, tp)), local_sem.at[2])
     own_shared = pltpu.make_async_copy(
-        shared_ref, shared.at[:, :, columns(gr, tp)], local_sem.at[3]
-    )
-    locals_ = (own_rows, own_slice, own_piece, own_shared)
+        shared_mine, shared.at[:, :, columns(gr, tp)], local_sem.at[3]
+    )
+    locals_ = (own_slice, own_piece, own_shared)
     for copy in locals_:
         copy.start()
-    lane = lax.broadcasted_iota(jnp.int32, select.shape, 0)
-    unit = lax.broadcasted_iota(jnp.int32, select.shape, 1)
-    first = (jnp.where(lane < LANES // 2, lane, lane - LANES // 2) - tp * n) * hidden_piece
-    inside = (unit >= first) & (unit < first + hidden_piece) & (unit < hidden)
-    select[...] = jnp.where(inside, 1.0, 0.0).astype(select.dtype)
 
     def take_rows(source):
         row_move(source, row_out_sem.at[source], row_sem.at[source], twin).wait_recv()
@@ -356,7 +420,7 @@
     for copy in locals_:
         copy.wait()
     far_columns = shared.at[:, :, columns(1 - gr, tp)]
-    remote(shared_ref, far_columns, shared_out_sem.at[0], shared_sem.at[0], across).wait_recv()
+    remote(shared_mine, far_columns, shared_out_sem.at[0], shared_sem.at[0], across).wait_recv()
     shared_relay = remote(far_columns, far_columns, shared_out_sem.at[2], shared_sem.at[2], twin)
     shared_relay.start()
     arrive_beside(outer, 0)
@@ -392,15 +456,10 @@
     column_send(fs).start()
 
     remote(
-        shared_ref, shared.at[:, :, columns(gr, other)], shared_out_sem.at[1], shared_sem.at[1], twin
+        shared_mine, shared.at[:, :, columns(gr, other)], shared_out_sem.at[1], shared_sem.at[1], twin
     ).wait_recv()
     last_columns = shared.at[:, :, columns(1 - gr, other)]
-    remote(shared_ref, last_columns, shared_out_sem.at[2], shared_sem.at[2], twin).wait_recv()
-    outs = []
-    for j, ref in enumerate((shared_gate_ref, shared_up_ref, shared_down_ref)):
-        outs.append(pltpu.make_async_copy(shared.at[j], ref, out_sem.at[3 + j]))
-    for copy in outs:
-        copy.start()
+    remote(shared_mine, last_columns, shared_out_sem.at[2], shared_sem.at[2], twin).wait_recv()
     tail = pltpu.make_async_copy(
         shared.at[:, pl.ds(pl.multiple_of(tp * extra, extra), extra), :],
         weights.at[:, pl.ds(hidden, extra), :],
@@ -529,10 +588,6 @@
             column_sem.at[source],
             across,
         ).wait_recv()
-    for j, ref in enumerate((gate_ref, up_ref, down_ref)):
-        copy = pltpu.make_async_copy(owned.at[j], ref.at[0], out_sem.at[j])
-        copy.start()
-        outs.append(copy)
 
     add_both(depth - 1)
     for j in range(depth - 1):
@@ -591,8 +646,6 @@
         side_send(j).wait_send()
     for j in range(depth - 1):
         sum_send(j).wait_send()
-    for copy in outs:
-        copy.wait()
 
 
 def direct_body(
@@ -607,54 +660,38 @@
     shared_up_trained,
     shared_down_trained,
 ):
-    gain_row = norm_gain[None, None, :]
+    n = lax.axis_size("fs")
     experts, hidden_piece, width = gate_trained.shape
-    pieces = (
-        jnp.stack([gate_trained * gain_row, up_trained * gain_row, down_trained], axis=0)
-        .astype(jnp.bfloat16)
-        .reshape(3, experts * hidden_piece, width)
-    )
-    shared_gain = norm_gain[None, :]
-    shared_stack = jnp.stack(
-        [shared_gate_trained * shared_gain, shared_up_trained * shared_gain, shared_down_trained],
-        axis=0,
-    ).astype(jnp.bfloat16)
-    values = tokens.astype(jnp.float32)
-    normed = (
-        values * lax.rsqrt(jnp.mean(values * values, axis=1, keepdims=True) + epsilon)
-    ).astype(jnp.bfloat16)
-    n = lax.axis_size("fs")
-    row_count, features = normed.shape
-    shared_piece = shared_stack.shape[1]
-    numbers = jnp.arange(LANES // 2, dtype=jnp.int32)
-    factors = jnp.sum(
-        jnp.where(routes[:, :, None] == numbers, route_weights[:, :, None], 0.0), axis=1
-    )
-    high = lax.reduce_precision(factors, 8, 7)
-    rows = jnp.concatenate(
-        [normed, high.astype(jnp.bfloat16), (factors - high).astype(jnp.bfloat16)], axis=1
-    )
+    row_count, features = tokens.shape
+    shared_piece = shared_gate_trained.shape[0]
+    stacked = (experts * hidden_piece, width)
     hidden = n * hidden_piece
     hidden_all = hidden + shared_piece // 2
     vmem = pl.BlockSpec(memory_space=pltpu.VMEM)
-    hbm = pl.BlockSpec(memory_space=pl.ANY)
+    hbm = pl.BlockSpec(memory_space=pltpu.HBM)
     kind = jnp.bfloat16
-    expert_shape = jax.ShapeDtypeStruct((1, hidden, features), kind)
-    shared_shape = jax.ShapeDtypeStruct((shared_piece, features), kind)
     DMA = pltpu.SemaphoreType.DMA
-    return pl.pallas_call(
+    combined, owned, shared = pl.pallas_call(
         functools.partial(exchange_kernel, n),
-        out_shape=(jax.ShapeDtypeStruct((row_count, features), kind),)
-        + (expert_shape,) * 3
-        + (shared_shape,) * 3,
-        in_specs=[vmem] * 3,
-        out_specs=(vmem,) + (hbm,) * 6,
+        out_shape=(
+            jax.ShapeDtypeStruct((row_count, features), kind),
+            jax.ShapeDtypeStruct((3, hidden, features), kind),
+            jax.ShapeDtypeStruct((3, shared_piece, features), kind),
+        ),
+        in_specs=[hbm] * 10,
+        out_specs=(vmem,) * 3,
         scratch_shapes=[
             pltpu.VMEM((3, hidden_all, features), kind),
-            pltpu.VMEM((3, hidden, features), kind),
-            pltpu.VMEM((3, shared_piece, features), kind),
             pltpu.VMEM((experts * row_count, features + LANES), kind),
             pltpu.VMEM((LANES, hidden_all), kind),
+            pltpu.VMEM((row_count, features), kind),
+            pltpu.VMEM(routes.shape[::-1], jnp.int32),
+            pltpu.VMEM(routes.shape[::-1], jnp.float32),
+            pltpu.VMEM((1, width), jnp.float32),
+            pltpu.VMEM((3, shared_piece, width), jnp.float32),
+            pltpu.VMEM((3,) + stacked, jnp.float32),
+            pltpu.VMEM((3,) + stacked, kind),
+            pltpu.VMEM((3, shared_piece, width), kind),
             pltpu.VMEM((n, 2 * row_count, features), kind),
             pltpu.VMEM((n, row_count, features), kind),
             pltpu.VMEM((n, row_count, features), kind),
@@ -681,12 +718,55 @@
             DMA((n // 2,)),
             DMA((n // 2 - 1,)),
             DMA((n // 2 - 1,)),
-            DMA((6,)),
+            DMA((3, 2)),
+            DMA((7,)),
         ],
         compiler_params=pltpu.CompilerParams(
-            collective_id=0, has_side_effects=True, vmem_limit_bytes=60 * 1024 * 1024
+            collective_id=0, has_side_effects=True, vmem_limit_bytes=48 * 1024 * 1024
         ),
-    )(pieces, shared_stack, rows)
+    )(*[
+        pltpu.with_memory_space_constraint(array, pltpu.HBM)
+        for array in (
+            tokens,
+            routes.T,
+            route_weights.T,
+            norm_gain[None, :],
+            gate_trained.reshape(stacked),
+            up_trained.reshape(stacked),
+            down_trained.reshape(stacked),
+            shared_gate_trained,
+            shared_up_trained,
+            shared_down_trained,
+        )
+    ])
+    return settle(combined, owned, shared)
+
+
+def settle_kernel(combined_ref, owned_ref, shared_ref, combined_out, *refs):
+    sems = refs[-1]
+    copies = [pltpu.make_async_copy(combined_ref, combined_out, sems.at[6])]
+    for j in range(3):
+        copies.append(pltpu.make_async_copy(owned_ref.at[j], refs[j].at[0], sems.at[j]))
+        copies.append(pltpu.make_async_copy(shared_ref.at[j], refs[3 + j], sems.at[3 + j]))
+    for copy in copies:
+        copy.start()
+    for copy in copies:
+        copy.wait()
+
+
+def settle(combined, owned, shared):
+    expert_shape = jax.ShapeDtypeStruct((1,) + owned.shape[1:], owned.dtype)
+    shared_shape = jax.ShapeDtypeStruct(shared.shape[1:], shared.dtype)
+    return pl.pallas_call(
+        settle_kernel,
+        out_shape=(jax.ShapeDtypeStruct(combined.shape, combined.dtype),)
+        + (expert_shape,) * 3
+        + (shared_shape,) * 3,
+        in_specs=[pl.BlockSpec(memory_space=pltpu.VMEM)] * 3,
+        out_specs=(pl.BlockSpec(memory_space=pltpu.HBM),) * 7,
+        scratch_shapes=[pltpu.SemaphoreType.DMA((7,))],
+        compiler_params=pltpu.CompilerParams(vmem_limit_bytes=8 * 1024 * 1024),
+    )(combined, owned, shared)
 
 
 def body(*arguments):

time: 167 us -> 150 us (0.90)
  local copies, waits for them, and re-layouts: 12.4 us -> 0 us
  other arithmetic: 7.75 us -> 0 us
  Pallas kernels: 146 us -> 149 us
    unnamed x25 -> x0, local copies, waits for them, and re-layouts: 11.3 us -> none
    another operation x5 -> x0, other arithmetic: 5.53 us -> none
    pallas_call x0 -> x1, Pallas kernels: none -> 2.62 us  [settle(): pl.pallas_call(settle_kernel, out_shape=(jax.ShapeDtypeStruct(combined.sh...]
    reduce_sum x2 -> x0, other arithmetic: 2.04 us -> none  [the longest x1 1.29 us: direct_body(): jnp.mean(values * values, axis=1, keepdims=True) + epsilon]
where the time goes in v2:
time: 150 us
  Pallas kernels  149 us (99%)
    pallas_call x1, Pallas kernels, direct_body(): pl.pallas_call(functools.partial(exchange_kernel, n), out_shape=(jax.Shap...  147 us

profile of v2, /device:TPU:0, one launch (start us, length us, event | category | flops | bytes accessed | tf_op | source)
XLA Modules:
  0.0 150.0 jit_solution(5148631654041142669)
XLA Ops:
  0.6 146.8 %shard_map.153 = (bf16[128,2048]{1,0:T(8,128)(2,1)S(1)}, bf16[3,384,2048]{2,1,0:T(8,128)(2,1)S(1)}, bf16[3,64,2048]{2,1,0:T(8,128)(2,1)S(1)}) custom-call(bf16[128,2048]{1,0:T(8,128)(2,1)} %tokens_hbm.1, s32[8,128]{1,0:T(8,128)} %bitcast.9, f32[8,128]{1,0:T(8,128)} %bitcast.10, f32[1,512]{1,0:T(1,128)} %bitcast.11, f32[768,512]{1,0:T(8,128)} %bitcast.6, ...), custom_call_target="tpu_custom_call" | custom-call | tf_op jit(solution)/shard_map/pallas_call | solution.py:674
  147.4 2.6 %shard_map.154 = (bf16[128,2048]{1,0:T(8,128)(2,1)}, bf16[1,384,2048]{2,1,0:T(8,128)(2,1)}, bf16[1,384,2048]{2,1,0:T(8,128)(2,1)}, bf16[1,384,2048]{2,1,0:T(8,12...) custom-call(bf16[128,2048]{1,0:T(8,128)(2,1)S(1)} %get-tuple-element.10.combined_ref, ...), custom_call_target="tpu_custom_call" | custom-call | tf_op jit(solution)/shard_map/pallas_call | solution.py:760

commit v3 on v2

--- a/solution.py
+++ b/solution.py
@@ -126,16 +126,21 @@
     shared_stage,
     stage,
     pieces,
+    guests,
     shared_mine,
     parts,
     pair_in,
     sums,
     side_in,
+    mate_in,
     sums_in,
     local_sem,
     slice_out_sem,
     slice_sem,
     piece_sem,
+    guest_out_sem,
+    guest_sem,
+    guest_on_sem,
     weight_sem,
     column_out_sem,
     column_sem,
@@ -145,6 +150,9 @@
     row_side_sem,
     row_back_sem,
     row_sem,
+    mix_out_sem,
+    mix_back_sem,
+    mix_sem,
     row_pair_out_sem,
     row_pair_sem,
     part_sem,
@@ -152,6 +160,7 @@
     side_sem,
     side_recv_sem,
     sum_sem,
+    mate_sem,
     sum_recv_sem,
     stage_sem,
     input_sem,
@@ -277,6 +286,17 @@
         start = pl.multiple_of((source * 2 + t) * row_count, row_count)
         return rows.at[pl.ds(start, row_count)]
 
+    late = row_count // 4
+    early = row_count - late
+
+    def row_early(source):
+        start = pl.multiple_of((source * 2 + tp) * row_count, row_count)
+        return rows.at[pl.ds(start, early)]
+
+    def row_late(source):
+        start = pl.multiple_of((source * 2 + tp) * row_count, row_count)
+        return rows.at[pl.ds(pl.multiple_of(start + early, late), late)]
+
     def nearby(k):
         place = lax.rem(outer + toward * lax.div(k, 2) + depth, depth)
         return place * 2 + jnp.where(lax.rem(k, 2) == 0, inner, 1 - inner)
@@ -298,6 +318,38 @@
             (gr, d, t),
         )
 
+    pair = 2 * hidden_piece
+
+    def guest_send(place):
+        start = pl.multiple_of((place * 2 + 1 - inner) * pair, 16)
+        spot = pl.ds(place * pair, pair)
+        return remote(
+            pieces.at[:, pl.ds(start, pair), :],
+            guests.at[:, spot, :],
+            guest_out_sem.at[place],
+            guest_sem.at[place],
+            beside,
+        )
+
+    fs_beside = outer * 2 + 1 - inner
+
+    def guest(place, t):
+        start = pl.multiple_of(place * pair + t * hidden_piece, 16)
+        return guests.at[:, pl.ds(start, hidden_piece), :]
+
+    def guest_onward(place, t):
+        return remote(
+            guest(place, t),
+            slab(fs_beside, columns(gr, tp)),
+            guest_on_sem.at[place, t],
+            weight_sem.at[fs_beside, tp],
+            (gr, place * 2 + inner, t),
+        )
+
+    guest_local = pltpu.make_async_copy(
+        guest(outer, tp), slab(fs_beside, columns(gr, tp)), local_sem.at[0]
+    )
+
     def column_send(source):
         return remote(
             slab(source, half),
@@ -318,8 +370,17 @@
             (gr, (outer + step) * 2 + inner, tp),
         )
 
-    def row_beside(source):
-        return row_move(source, row_side_sem.at[lax.div(source, 2)], row_sem.at[source], beside)
+    def row_beside(source, distance):
+        block = row_early(source) if distance < depth - 1 else row_block(source, tp)
+        return remote(block, block, row_side_sem.at[lax.div(source, 2)], row_sem.at[source], beside)
+
+    def mixed(place, send, step):
+        block = row_late(place * 2 + 1 - inner)
+        device = (gr, (outer + step) * 2 + inner, tp)
+        return remote(block, block, send, mix_sem.at[place], device)
+
+    mix_up = mixed(outer, mix_out_sem.at[outer], 1)
+    mix_back = mixed(outer, mix_back_sem.at[0], -1)
 
     def row_relay(source):
         return row_move(source, row_pair_out_sem.at[source], row_pair_sem.at[source], twin)
@@ -330,12 +391,12 @@
     own_relay = row_move(fs, row_pair_out_sem.at[fs], row_pair_sem.at[fs], twin)
 
     def at_distance(distance, action):
-        for step in (1, -1):
+        for step in (-1, 1):
             place = outer - step * distance
 
             @pl.when((place >= 0) & (place < depth))
             def _():
-                action(place, step)
+                action(place, step, distance)
 
     def onward_exists(step):
         return (outer + step >= 0) & (outer + step < depth)
@@ -367,22 +428,13 @@
     twin_piece = piece_send(fs, other)
     twin_piece.start()
 
-    def ship(step, distances):
-        for distance in distances:
-            place = outer + step * distance
-
-            @pl.when((place >= 0) & (place < depth))
+    def ship(places):
+        for place in places:
+
+            @pl.when(place != outer)
             def _():
                 piece_send(place * 2 + inner, 0).start()
                 piece_send(place * 2 + inner, 1).start()
-
-    @pl.when(outer == 0)
-    def _():
-        ship(1, (1,))
-
-    @pl.when(outer == depth - 1)
-    def _():
-        ship(-1, (1,))
 
     own_slice = pltpu.make_async_copy(portion(tp), sliced(gr, tp), local_sem.at[1])
     own_piece = pltpu.make_async_copy(piece(expert), slab(fs, columns(gr, tp)), local_sem.at[2])
@@ -396,7 +448,7 @@
     def take_rows(source):
         row_move(source, row_out_sem.at[source], row_sem.at[source], twin).wait_recv()
 
-    def arrive(place, step):
+    def arrive(place, step, distance):
         source = place * 2 + inner
         take_rows(source)
 
@@ -404,44 +456,61 @@
         def _():
             row_onward(source, step).start()
 
-        row_beside(source).start()
+        row_beside(source, distance).start()
         row_relay(source).start()
 
-        @pl.when(place == (0 if step == 1 else depth - 1))
-        def _():
-            ship(step, range(1, depth))
-
-    def arrive_beside(place, step):
+    def arrive_mixed(place, step, distance):
+        mixed(place, mix_out_sem.at[place], step).wait_recv()
+        if distance < depth - 2:
+
+            @pl.when(onward_exists(step))
+            def _():
+                mixed(place, mix_out_sem.at[place], step).start()
+
+    def arrive_beside(place, step, distance):
         source = place * 2 + 1 - inner
-        take_rows(source)
+        row_beside(source, distance).wait_recv()
         row_relay(source).start()
 
     at_distance(1, arrive)
+    take_rows(outer * 2 + 1 - inner)
+
+    @pl.when(outer < depth - 1)
+    def _():
+        mix_up.start()
+
+    @pl.when(outer > 0)
+    def _():
+        mix_back.start()
+
+    row_relay(outer * 2 + 1 - inner).start()
+    for place in range(depth):
+        guest_send(place).start()
     for copy in locals_:
         copy.wait()
     far_columns = shared.at[:, :, columns(1 - gr, tp)]
     remote(shared_mine, far_columns, shared_out_sem.at[0], shared_sem.at[0], across).wait_recv()
     shared_relay = remote(far_columns, far_columns, shared_out_sem.at[2], shared_sem.at[2], twin)
     shared_relay.start()
-    arrive_beside(outer, 0)
-    for distance in range(2, depth):
-        at_distance(distance, arrive)
-        if distance == 2:
-
-            @pl.when(outer == 0)
-            def _():
-                ship(1, range(2, depth))
-
-            @pl.when(outer == depth - 1)
-            def _():
-                ship(-1, range(2, depth))
-
-        at_distance(distance - 1, arrive_beside)
-
-    for k in range(1, n, 2):
-        d = nearby(k)
-        piece_send(d, 0).start()
-        piece_send(d, 1).start()
+    at_distance(2, arrive)
+    ship(range(1, depth - 1))
+    at_distance(1, arrive_mixed)
+    at_distance(1, arrive_beside)
+    at_distance(3, arrive)
+    at_distance(2, arrive_mixed)
+    ship((0, depth - 1))
+
+    for place in range(depth):
+        guest_send(place).wait_recv()
+
+        @pl.when(place != outer)
+        def _():
+            guest_onward(place, 0).start()
+            guest_onward(place, 1).start()
+
+    guest_onward(outer, other).start()
+    guest_local.start()
+    guest_local.wait()
 
     def take_twin_piece(source, t):
         remote(
@@ -482,23 +551,36 @@
             twin,
         )
 
+    low = outer < depth // 2
+    near = jnp.where(low, 1, 2 * depth - 3) - outer
+    at_end = (outer == 0) | (outer == depth - 1)
+
     def place_of(j):
-        return lax.rem(outer + toward * (j + 1) + depth, depth)
+        far = jnp.where(low, depth // 2 + j, depth // 2 - 1 - j)
+        return jnp.where(j < depth // 2, far, jnp.where(j == depth - 1, outer, near))
 
     def side_send(j):
         return remote(
             sums.at[2 * j], side_in.at[j], side_sem.at[j], side_recv_sem.at[j], beside
         )
 
+    def mate_send(j):
+        return remote(
+            sums.at[2 * j + 1],
+            mate_in.at[j],
+            sum_sem.at[j],
+            mate_sem.at[j],
+            (gr, near * 2 + inner, tp),
+        )
+
     def sum_send(j):
-        place = place_of(j)
-        slot = lax.rem(outer - place + 2 * depth - 1, depth)
+        slot = 1 if j < depth // 2 else 0
         return remote(
             sums.at[2 * j + 1],
             sums_in.at[slot],
             sum_sem.at[j],
             sum_recv_sem.at[slot],
-            (gr, place * 2 + inner, tp),
+            (gr, place_of(j) * 2 + inner, tp),
         )
 
     chunk = 32
@@ -514,10 +596,12 @@
             value = value + pair_in[k, pl.ds(at, chunk), :].astype(jnp.float32)
             sums[k, pl.ds(at, chunk), :] = value.astype(jnp.bfloat16)
 
-    def add_both(j):
+    def await_both(j):
+        part_send(2 * j + 1).wait_recv()
+        side_send(j).wait_recv()
+
+    def add_both(j, mate):
         k = 2 * j + 1
-        part_send(k).wait_recv()
-        side_send(j).wait_recv()
 
         @pl.loop(0, row_count // chunk)
         def _(i):
@@ -526,6 +610,8 @@
             value = parts[k, pl.ds(mine, chunk), :].astype(jnp.float32)
             value = value + pair_in[k, pl.ds(at, chunk), :].astype(jnp.float32)
             value = value + side_in[j, pl.ds(at, chunk), :].astype(jnp.float32)
+            if mate:
+                value = value + mate_in[j, pl.ds(at, chunk), :].astype(jnp.float32)
             sums[k, pl.ds(at, chunk), :] = value.astype(jnp.bfloat16)
 
     def take_weights(source):
@@ -533,14 +619,37 @@
         take_twin_piece(source, 1)
         column_send(source).start()
 
+    def pass_far(j):
+        await_both(j)
+
+        @pl.when(at_end)
+        def _():
+            add_both(j, False)
+            mate_send(j).start()
+
+        @pl.when(jnp.logical_not(at_end))
+        def _():
+            mate_send(j).wait_recv()
+            add_both(j, True)
+            sum_send(j).start()
+
+    def pass_near(j):
+        await_both(j)
+        add_both(j, False)
+        sum_send(j).start()
+
     @pl.loop(0, n)
     def _(k):
         j = lax.div(k, 2)
         d = place_of(j) * 2 + jnp.where(lax.rem(k, 2) == 0, 1 - inner, inner)
 
-        @pl.when(k == n - 4)
-        def _():
-            at_distance(depth - 1, arrive_beside)
+        @pl.when(k == jnp.where(at_end, 0, 2))
+        def _():
+            at_distance(2, arrive_beside)
+
+        @pl.when(k == 2)
+        def _():
+            at_distance(3, arrive_beside)
 
         remote(
             row_block(d, other), row_block(d, other), row_pair_out_sem.at[d], row_pair_sem.at[d], twin
@@ -573,11 +682,27 @@
         def _():
             take_weights(nearby(2 * k))
 
-    take_weights(nearby(1))
-    for j in range(depth - 1):
-        take_weights(nearby(2 * j + 3))
-        add_both(j)
-        sum_send(j).start()
+        @pl.when((k == n - 3) & at_end)
+        def _():
+            pass_far(0)
+
+    take_twin_piece(fs_beside, other)
+    column_send(fs_beside).start()
+
+    @pl.when(jnp.logical_not(at_end))
+    def _():
+        pass_far(0)
+        pass_near(2)
+
+    take_weights(nearby(3))
+    pass_far(1)
+    take_weights(nearby(5))
+
+    @pl.when(at_end)
+    def _():
+        pass_near(2)
+
+    take_weights(nearby(7))
 
     for k in range(n):
         source = nearby(k)
@@ -589,25 +714,28 @@
             across,
         ).wait_recv()
 
-    add_both(depth - 1)
-    for j in range(depth - 1):
+    await_both(depth - 1)
+    add_both(depth - 1, False)
+    for j in range(2):
         remote(sums.at[0], sums_in.at[j], sum_sem.at[j], sum_recv_sem.at[j], twin).wait_recv()
 
     @pl.loop(0, row_count // chunk)
     def _(i):
         at = pl.ds(pl.multiple_of(i * chunk, chunk), chunk)
         total = sums[n - 1, at, :].astype(jnp.float32)
-        for j in range(depth - 1):
+        for j in range(2):
             total = total + sums_in[j, at, :].astype(jnp.float32)
         combined_ref[at, :] = total.astype(jnp.bfloat16)
 
     @pl.when(outer < depth - 1)
     def _():
         own_up.wait_send()
+        mix_up.wait_send()
 
     @pl.when(outer > 0)
     def _():
         own_back.wait_send()
+        mix_back.wait_send()
 
     for copy in (
         own_beside,
@@ -622,24 +750,34 @@
     ):
         copy.wait_send()
 
-    def sent(place, step):
+    def sent(place, step, distance):
         source = place * 2 + inner
 
         @pl.when(onward_exists(step))
         def _():
             row_onward(source, step).wait_send()
-
-        row_beside(source).wait_send()
+            if distance < depth - 2:
+                mixed(place, mix_out_sem.at[place], step).wait_send()
+
+        row_beside(source, distance).wait_send()
 
     for distance in range(1, depth):
         at_distance(distance, sent)
     column_send(fs).wait_send()
     for k in range(1, n):
         d = lax.rem(fs + k, n)
-        piece_send(d, 0).wait_send()
-        piece_send(d, 1).wait_send()
         column_send(d).wait_send()
         row_relay(d).wait_send()
+    for place in range(depth):
+        guest_send(place).wait_send()
+
+        @pl.when(place != outer)
+        def _():
+            for t in range(2):
+                piece_send(place * 2 + inner, t).wait_send()
+                guest_onward(place, t).wait_send()
+
+    guest_onward(outer, other).wait_send()
     for k in range(n):
         part_send(k).wait_send()
     for j in range(depth):
@@ -691,16 +829,21 @@
             pltpu.VMEM((3, shared_piece, width), jnp.float32),
             pltpu.VMEM((3,) + stacked, jnp.float32),
             pltpu.VMEM((3,) + stacked, kind),
+            pltpu.VMEM((3, n * hidden_piece, width), kind),
             pltpu.VMEM((3, shared_piece, width), kind),
             pltpu.VMEM((n, 2 * row_count, features), kind),
             pltpu.VMEM((n, row_count, features), kind),
             pltpu.VMEM((n, row_count, features), kind),
             pltpu.VMEM((n // 2, row_count, features), kind),
-            pltpu.VMEM((n // 2 - 1, row_count, features), kind),
+            pltpu.VMEM((n // 4, row_count, features), kind),
+            pltpu.VMEM((2, row_count, features), kind),
             DMA((5,)),
             DMA((3,)),
             DMA((3,)),
             DMA((n, 2)),
+            DMA((n // 2,)),
+            DMA((n // 2,)),
+            DMA((n // 2, 2)),
             DMA((n, 2)),
             DMA((n,)),
             DMA((n,)),
@@ -710,6 +853,9 @@
             DMA((n // 2,)),
             DMA((1,)),
             DMA((n,)),
+            DMA((n // 2,)),
+            DMA((1,)),
+            DMA((n // 2,)),
             DMA((n,)),
             DMA((n,)),
             DMA((n,)),
@@ -717,7 +863,8 @@
             DMA((n // 2,)),
             DMA((n // 2,)),
             DMA((n // 2 - 1,)),
-            DMA((n // 2 - 1,)),
+            DMA((n // 4,)),
+            DMA((2,)),
             DMA((3, 2)),
             DMA((7,)),
         ],
@@ -773,7 +920,7 @@
     experts = lax.axis_size("fs") * lax.axis_size("tp")
     per_token = arguments[1].shape[1]
     pairs = lax.axis_size("gr") == 2 and lax.axis_size("tp") == 2
-    if pairs and lax.axis_size("fs") % 2 == 0 and experts <= min(2 * per_token, LANES // 2):
+    if pairs and lax.axis_size("fs") == 8 and experts <= min(2 * per_token, LANES // 2):
         return direct_body(*arguments)
     return dispatch_body(*arguments)
 

time: 150 us -> 136 us (0.907)
  Pallas kernels: 149 us -> 135 us
    pallas_call x1, Pallas kernels: 147 us -> 133 us  [direct_body(): pl.pallas_call(functools.partial(exchange_kernel, n), out_shape=(jax.Shap...]
where the time goes in v3:
time: 136 us
  Pallas kernels  135 us (99%)
    pallas_call x1, Pallas kernels, direct_body(): pl.pallas_call(functools.partial(exchange_kernel, n), out_shape=(jax.Shap...  133 us

profile of v3, /device:TPU:0, one launch (start us, length us, event | category | flops | bytes accessed | tf_op | source)
XLA Modules:
  0.0 136.0 jit_solution(9583031743708422097)
XLA Ops:
  0.6 132.7 %shard_map.153 = (bf16[128,2048]{1,0:T(8,128)(2,1)S(1)}, bf16[3,384,2048]{2,1,0:T(8,128)(2,1)S(1)}, bf16[3,64,2048]{2,1,0:T(8,128)(2,1)S(1)}) custom-call(bf16[128,2048]{1,0:T(8,128)(2,1)} %tokens_hbm.1, s32[8,128]{1,0:T(8,128)} %bitcast.9, f32[8,128]{1,0:T(8,128)} %bitcast.10, f32[1,512]{1,0:T(1,128)} %bitcast.11, f32[768,512]{1,0:T(8,128)} %bitcast.6, ...), custom_call_target="tpu_custom_call" | custom-call | tf_op jit(solution)/shard_map/pallas_call | solution.py:812
  133.4 2.6 %shard_map.154 = (bf16[128,2048]{1,0:T(8,128)(2,1)}, bf16[1,384,2048]{2,1,0:T(8,128)(2,1)}, bf16[1,384,2048]{2,1,0:T(8,128)(2,1)}, bf16[1,384,2048]{2,1,0:T(8,12...) custom-call(bf16[128,2048]{1,0:T(8,128)(2,1)S(1)} %get-tuple-element.10.combined_ref, ...), custom_call_target="tpu_custom_call" | custom-call | tf_op jit(solution)/shard_map/pallas_call | solution.py:907

commit v4 on v3

--- a/solution.py
+++ b/solution.py
@@ -197,13 +197,6 @@
     ):
         inputs_in.append(pltpu.make_async_copy(source, target, input_sem.at[i]))
         inputs_in[i].start()
-    staged = {}
-    for t in (0, 1):
-        for j, ref in enumerate((gate_hbm, up_hbm, down_hbm)):
-            part = pl.ds(t * hidden, hidden)
-            staged[j, t] = pltpu.make_async_copy(ref.at[part], stage.at[j, part], stage_sem.at[j, t])
-            staged[j, t].start()
-
     barrier = pltpu.get_barrier_semaphore()
     for device in (across, across_twin, twin):
         pl.semaphore_signal(barrier, inc=1, device_id=device, device_id_type=MESH)
@@ -215,8 +208,13 @@
 
     own_start = pl.multiple_of(expert * row_count, row_count)
     few = 16
-    for copy in inputs_in:
-        copy.wait()
+    inputs_in[0].wait()
+    staged = {}
+    for t in (0, 1):
+        for j, ref in enumerate((gate_hbm, up_hbm, down_hbm)):
+            part = pl.ds(t * hidden, hidden)
+            staged[j, t] = pltpu.make_async_copy(ref.at[part], stage.at[j, part], stage_sem.at[j, t])
+            staged[j, t].start()
 
     @pl.loop(0, row_count // few)
     def _(i):
@@ -226,6 +224,8 @@
         normed = (values * lax.rsqrt(mean + epsilon)).astype(jnp.bfloat16)
         rows[pl.ds(own_start + at, few), 0:features] = normed
 
+    for copy in inputs_in[1:]:
+        copy.wait()
     number = lax.broadcasted_iota(jnp.int32, (LANES // 2, row_count), 0)
     factors = jnp.zeros(number.shape, jnp.float32)
     for k in range(routes_ref.shape[0]):
@@ -235,25 +235,6 @@
     both = jnp.concatenate([high, factors - high], axis=0)
     rows[pl.ds(own_start, row_count), features : features + LANES] = both.T.astype(jnp.bfloat16)
 
-    gain = gain_ref[...]
-    for j in range(3):
-        value = shared_stage[j] if j == 2 else shared_stage[j] * gain
-        shared_mine[j] = value.astype(jnp.bfloat16)
-    for t in (0, 1):
-        for j in range(3):
-            staged[j, t].wait()
-
-            @pl.loop(0, n)
-            def _(i):
-                at = pl.ds(pl.multiple_of((t * n + i) * hidden_piece, hidden_piece), hidden_piece)
-                value = stage[j, at, :] if j == 2 else stage[j, at, :] * gain_ref[...]
-                pieces[j, at, :] = value.astype(jnp.bfloat16)
-
-    lane = lax.broadcasted_iota(jnp.int32, select.shape, 0)
-    unit = lax.broadcasted_iota(jnp.int32, select.shape, 1)
-    first = (jnp.where(lane < LANES // 2, lane, lane - LANES // 2) - tp * n) * hidden_piece
-    inside = (unit >= first) & (unit < first + hidden_piece) & (unit < hidden)
-    select[...] = jnp.where(inside, 1.0, 0.0).astype(select.dtype)
     pl.semaphore_wait(barrier, 2 * n + 1)
 
     def remote(src, dst, send, recv, device):
@@ -286,7 +267,7 @@
         start = pl.multiple_of((source * 2 + t) * row_count, row_count)
         return rows.at[pl.ds(start, row_count)]
 
-    late = row_count // 4
+    late = row_count * 3 // 8
     early = row_count - late
 
     def row_early(source):
@@ -295,7 +276,7 @@
 
     def row_late(source):
         start = pl.multiple_of((source * 2 + tp) * row_count, row_count)
-        return rows.at[pl.ds(pl.multiple_of(start + early, late), late)]
+        return rows.at[pl.ds(pl.multiple_of(start + early, 16), late)]
 
     def nearby(k):
         place = lax.rem(outer + toward * lax.div(k, 2) + depth, depth)
@@ -410,6 +391,26 @@
         own_back.start()
 
     own_beside.start()
+    own_relay.start()
+    gain = gain_ref[...]
+    for j in range(3):
+        value = shared_stage[j] if j == 2 else shared_stage[j] * gain
+        shared_mine[j] = value.astype(jnp.bfloat16)
+    for t in (0, 1):
+        for j in range(3):
+            staged[j, t].wait()
+
+            @pl.loop(0, n)
+            def _(i):
+                at = pl.ds(pl.multiple_of((t * n + i) * hidden_piece, hidden_piece), hidden_piece)
+                value = stage[j, at, :] if j == 2 else stage[j, at, :] * gain_ref[...]
+                pieces[j, at, :] = value.astype(jnp.bfloat16)
+
+    lane = lax.broadcasted_iota(jnp.int32, select.shape, 0)
+    unit = lax.broadcasted_iota(jnp.int32, select.shape, 1)
+    first = (jnp.where(lane < LANES // 2, lane, lane - LANES // 2) - tp * n) * hidden_piece
+    inside = (unit >= first) & (unit < first + hidden_piece) & (unit < hidden)
+    select[...] = jnp.where(inside, 1.0, 0.0).astype(select.dtype)
     shared_far = remote(
         shared_mine, shared.at[:, :, columns(gr, tp)], shared_out_sem.at[0], shared_sem.at[0], across
     )
@@ -419,7 +420,6 @@
     slice_twin = slice_send(2, other, twin)
     slice_far.start()
     slice_cross.start()
-    own_relay.start()
     slice_twin.start()
     shared_twin = remote(
         shared_mine, shared.at[:, :, columns(gr, tp)], shared_out_sem.at[1], shared_sem.at[1], twin
@@ -523,6 +523,8 @@
 
     take_twin_piece(fs, other)
     column_send(fs).start()
+    take_twin_piece(fs_beside, other)
+    column_send(fs_beside).start()
 
     remote(
         shared_mine, shared.at[:, :, columns(gr, other)], shared_out_sem.at[1], shared_sem.at[1], twin
@@ -559,54 +561,63 @@
         far = jnp.where(low, depth // 2 + j, depth // 2 - 1 - j)
         return jnp.where(j < depth // 2, far, jnp.where(j == depth - 1, outer, near))
 
-    def side_send(j):
+    steps = 2
+    span_rows = row_count // steps
+
+    def share(h):
+        return pl.ds(h * span_rows, span_rows)
+
+    def side_send(j, h):
         return remote(
-            sums.at[2 * j], side_in.at[j], side_sem.at[j], side_recv_sem.at[j], beside
-        )
-
-    def mate_send(j):
+            sums.at[2 * j, share(h)],
+            side_in.at[j, share(h)],
+            side_sem.at[j, h],
+            side_recv_sem.at[j, h],
+            beside,
+        )
+
+    def mate_send(j, h):
         return remote(
-            sums.at[2 * j + 1],
-            mate_in.at[j],
-            sum_sem.at[j],
-            mate_sem.at[j],
+            sums.at[2 * j + 1, share(h)],
+            mate_in.at[j, share(h)],
+            sum_sem.at[j, h],
+            mate_sem.at[j, h],
             (gr, near * 2 + inner, tp),
         )
 
-    def sum_send(j):
+    def sum_send(j, h):
         slot = 1 if j < depth // 2 else 0
         return remote(
-            sums.at[2 * j + 1],
-            sums_in.at[slot],
-            sum_sem.at[j],
-            sum_recv_sem.at[slot],
+            sums.at[2 * j + 1, share(h)],
+            sums_in.at[slot, share(h)],
+            sum_sem.at[j, h],
+            sum_recv_sem.at[slot, h],
             (gr, place_of(j) * 2 + inner, tp),
         )
 
     chunk = 32
 
-    def add_pair(k):
-        part_send(k).wait_recv()
-
-        @pl.loop(0, row_count // chunk)
+    def add_pair(k, h):
+        @pl.loop(0, span_rows // chunk)
         def _(i):
-            at = pl.multiple_of(i * chunk, chunk)
-            mine = pl.multiple_of(tp * row_count + i * chunk, chunk)
+            at = pl.multiple_of(h * span_rows + i * chunk, chunk)
+            mine = pl.multiple_of(tp * row_count + at, chunk)
             value = parts[k, pl.ds(mine, chunk), :].astype(jnp.float32)
             value = value + pair_in[k, pl.ds(at, chunk), :].astype(jnp.float32)
             sums[k, pl.ds(at, chunk), :] = value.astype(jnp.bfloat16)
 
-    def await_both(j):
-        part_send(2 * j + 1).wait_recv()
-        side_send(j).wait_recv()
-
-    def add_both(j, mate):
+    def await_both(j, h):
+        if h == 0:
+            part_send(2 * j + 1).wait_recv()
+        side_send(j, h).wait_recv()
+
+    def add_both(j, h, mate):
         k = 2 * j + 1
 
-        @pl.loop(0, row_count // chunk)
+        @pl.loop(0, span_rows // chunk)
         def _(i):
-            at = pl.multiple_of(i * chunk, chunk)
-            mine = pl.multiple_of(tp * row_count + i * chunk, chunk)
+            at = pl.multiple_of(h * span_rows + i * chunk, chunk)
+            mine = pl.multiple_of(tp * row_count + at, chunk)
             value = parts[k, pl.ds(mine, chunk), :].astype(jnp.float32)
             value = value + pair_in[k, pl.ds(at, chunk), :].astype(jnp.float32)
             value = value + side_in[j, pl.ds(at, chunk), :].astype(jnp.float32)
@@ -619,31 +630,35 @@
         take_twin_piece(source, 1)
         column_send(source).start()
 
-    def pass_far(j):
-        await_both(j)
+    def pass_far(j, h):
+        await_both(j, h)
 
         @pl.when(at_end)
         def _():
-            add_both(j, False)
-            mate_send(j).start()
+            add_both(j, h, False)
+            mate_send(j, h).start()
 
         @pl.when(jnp.logical_not(at_end))
         def _():
-            mate_send(j).wait_recv()
-            add_both(j, True)
-            sum_send(j).start()
+            mate_send(j, h).wait_recv()
+            add_both(j, h, True)
+            sum_send(j, h).start()
 
     def pass_near(j):
-        await_both(j)
-        add_both(j, False)
-        sum_send(j).start()
+        for h in range(steps):
+            await_both(j, h)
+            add_both(j, h, False)
+            sum_send(j, h).start()
 
     @pl.loop(0, n)
     def _(k):
-        j = lax.div(k, 2)
+        turn = lax.div(k, 2)
+        swapped = jnp.logical_not(at_end) & (turn > 0) & (turn < depth - 1)
+        j = jnp.where(swapped, depth - 1 - turn, turn)
+        item = 2 * j + lax.rem(k, 2)
         d = place_of(j) * 2 + jnp.where(lax.rem(k, 2) == 0, 1 - inner, inner)
 
-        @pl.when(k == jnp.where(at_end, 0, 2))
+        @pl.when(k == jnp.where(at_end, 0, 4))
         def _():
             at_distance(2, arrive_beside)
 
@@ -668,41 +683,52 @@
         units = (gate / (1.0 + jnp.exp(-gate)) * up * scale).astype(jnp.bfloat16)
         for c in range(4):
             span = pl.ds(c * width, width)
-            parts[k, :, span] = jnp.dot(
+            parts[item, :, span] = jnp.dot(
                 units, weights[2, :, span], preferred_element_type=jnp.float32
             ).astype(jnp.bfloat16)
-        part_send(k).start()
+        part_send(item).start()
 
         @pl.when(lax.rem(k, 2) == 1)
         def _():
-            add_pair(k - 1)
-            side_send(j).start()
-
-        @pl.when((k > 0) & (k < depth))
-        def _():
-            take_weights(nearby(2 * k))
-
-        @pl.when((k == n - 3) & at_end)
-        def _():
-            pass_far(0)
-
-    take_twin_piece(fs_beside, other)
-    column_send(fs_beside).start()
+            part_send(item - 1).wait_recv()
+            for h in range(steps):
+                add_pair(item - 1, h)
+                side_send(j, h).start()
+
+        @pl.when(k == 1)
+        def _():
+            take_weights(nearby(2))
+
+        @pl.when(k == 2)
+        def _():
+            take_weights(nearby(4))
+            take_weights(nearby(6))
+
+        @pl.when((k > depth) & (k < n - 1))
+        def _():
+            take_weights(nearby(2 * (k - depth) + 1))
+
+        for h in range(steps):
+
+            @pl.when((k == n - 4 + 2 * h // steps) & at_end)
+            def _():
+                pass_far(0, h)
 
     @pl.when(jnp.logical_not(at_end))
     def _():
-        pass_far(0)
         pass_near(2)
-
-    take_weights(nearby(3))
-    pass_far(1)
-    take_weights(nearby(5))
+        take_weights(nearby(n - 1))
+        for h in range(steps):
+            pass_far(0, h)
+
+    for h in range(steps):
+        pass_far(1, h)
 
     @pl.when(at_end)
     def _():
+        take_weights(nearby(n - 1))
         pass_near(2)
 
-    take_weights(nearby(7))
 
     for k in range(n):
         source = nearby(k)
@@ -714,18 +740,26 @@
             across,
         ).wait_recv()
 
-    await_both(depth - 1)
-    add_both(depth - 1, False)
-    for j in range(2):
-        remote(sums.at[0], sums_in.at[j], sum_sem.at[j], sum_recv_sem.at[j], twin).wait_recv()
-
-    @pl.loop(0, row_count // chunk)
-    def _(i):
-        at = pl.ds(pl.multiple_of(i * chunk, chunk), chunk)
-        total = sums[n - 1, at, :].astype(jnp.float32)
+    for h in range(steps):
+        await_both(depth - 1, h)
+        add_both(depth - 1, h, False)
+    for h in range(steps):
         for j in range(2):
-            total = total + sums_in[j, at, :].astype(jnp.float32)
-        combined_ref[at, :] = total.astype(jnp.bfloat16)
+            remote(
+                sums.at[0, share(h)],
+                sums_in.at[j, share(h)],
+                sum_sem.at[0, 0],
+                sum_recv_sem.at[j, h],
+                twin,
+            ).wait_recv()
+
+        @pl.loop(0, span_rows // chunk)
+        def _(i):
+            at = pl.ds(pl.multiple_of(h * span_rows + i * chunk, chunk), chunk)
+            total = sums[n - 1, at, :].astype(jnp.float32)
+            for j in range(2):
+                total = total + sums_in[j, at, :].astype(jnp.float32)
+            combined_ref[at, :] = total.astype(jnp.bfloat16)
 
     @pl.when(outer < depth - 1)
     def _():
@@ -780,10 +814,11 @@
     guest_onward(outer, other).wait_send()
     for k in range(n):
         part_send(k).wait_send()
-    for j in range(depth):
-        side_send(j).wait_send()
-    for j in range(depth - 1):
-        sum_send(j).wait_send()
+    for h in range(steps):
+        for j in range(depth):
+            side_send(j, h).wait_send()
+        for j in range(depth - 1):
+            sum_send(j, h).wait_send()
 
 
 def direct_body(
@@ -860,11 +895,11 @@
             DMA((n,)),
             DMA((n,)),
             DMA((n,)),
-            DMA((n // 2,)),
-            DMA((n // 2,)),
-            DMA((n // 2 - 1,)),
-            DMA((n // 4,)),
-            DMA((2,)),
+            DMA((n // 2, 2)),
+            DMA((n // 2, 2)),
+            DMA((n // 2 - 1, 2)),
+            DMA((n // 4, 2)),
+            DMA((2, 2)),
             DMA((3, 2)),
             DMA((7,)),
         ],

time: 136 us -> 128 us (0.941)
  Pallas kernels: 135 us -> 126 us
    pallas_call x1, Pallas kernels: 133 us -> 124 us  [direct_body(): pl.pallas_call(functools.partial(exchange_kernel, n), out_shape=(jax.Shap...]
where the time goes in v4:
time: 128 us; the launch traced here: 127 us
  Pallas kernels  126 us (98%)
    pallas_call x1, Pallas kernels, direct_body(): pl.pallas_call(functools.partial(exchange_kernel, n), out_shape=(jax.Shap...  124 us
    pallas_call x1, Pallas kernels, settle(): pl.pallas_call(settle_kernel, out_shape=(jax.ShapeDtypeStruct(combined.sh...  2.62 us

profile of v4, /device:TPU:0, one launch (start us, length us, event | category | flops | bytes accessed | tf_op | source)
XLA Modules:
  0.0 127.1 jit_solution(12622361732461067192)
XLA Ops:
  0.6 123.9 %shard_map.153 = (bf16[128,2048]{1,0:T(8,128)(2,1)S(1)}, bf16[3,384,2048]{2,1,0:T(8,128)(2,1)S(1)}, bf16[3,64,2048]{2,1,0:T(8,128)(2,1)S(1)}) custom-call(bf16[128,2048]{1,0:T(8,128)(2,1)} %tokens_hbm.1, s32[8,128]{1,0:T(8,128)} %bitcast.9, f32[8,128]{1,0:T(8,128)} %bitcast.10, f32[1,512]{1,0:T(1,128)} %bitcast.11, f32[768,512]{1,0:T(8,128)} %bitcast.6, ...), custom_call_target="tpu_custom_call" | custom-call | tf_op jit(solution)/shard_map/pallas_call | solution.py:847
  124.5 2.6 %shard_map.154 = (bf16[128,2048]{1,0:T(8,128)(2,1)}, bf16[1,384,2048]{2,1,0:T(8,128)(2,1)}, bf16[1,384,2048]{2,1,0:T(8,128)(2,1)}, bf16[1,384,2048]{2,1,0:T(8,12...) custom-call(bf16[128,2048]{1,0:T(8,128)(2,1)S(1)} %get-tuple-element.10.combined_ref, ...), custom_call_target="tpu_custom_call" | custom-call | tf_op jit(solution)/shard_map/pallas_call | solution.py:942

commit v5 on v4

--- a/solution.py
+++ b/solution.py
@@ -101,6 +101,23 @@
     return (combined, expert_gate, expert_up, expert_down, shared_gate, shared_up, shared_down)
 
 
+class Both:
+    def __init__(self, *copies):
+        self.copies = copies
+
+    def start(self):
+        for copy in self.copies:
+            copy.start()
+
+    def wait_recv(self):
+        for copy in self.copies:
+            copy.wait_recv()
+
+    def wait_send(self):
+        for copy in self.copies:
+            copy.wait_send()
+
+
 def exchange_kernel(
     n,
     tokens_hbm,
@@ -118,6 +135,7 @@
     shared,
     weights,
     rows,
+    table,
     select,
     tokens_ref,
     routes_ref,
@@ -222,18 +240,18 @@
         values = tokens_ref[pl.ds(at, few), :].astype(jnp.float32)
         mean = jnp.mean(values * values, axis=1, keepdims=True)
         normed = (values * lax.rsqrt(mean + epsilon)).astype(jnp.bfloat16)
-        rows[pl.ds(own_start + at, few), 0:features] = normed
+        rows[pl.ds(own_start + at, few), :] = normed
 
     for copy in inputs_in[1:]:
         copy.wait()
-    number = lax.broadcasted_iota(jnp.int32, (LANES // 2, row_count), 0)
+    number = lax.broadcasted_iota(jnp.int32, (2 * n, row_count), 0)
     factors = jnp.zeros(number.shape, jnp.float32)
     for k in range(routes_ref.shape[0]):
         named = routes_ref[k : k + 1, :] == number
         factors = factors + jnp.where(named, route_weights_ref[k : k + 1, :], 0.0)
     high = factors.astype(jnp.bfloat16).astype(jnp.float32)
     both = jnp.concatenate([high, factors - high], axis=0)
-    rows[pl.ds(own_start, row_count), features : features + LANES] = both.T.astype(jnp.bfloat16)
+    table[expert] = both.astype(jnp.bfloat16)
 
     pl.semaphore_wait(barrier, 2 * n + 1)
 
@@ -267,7 +285,7 @@
         start = pl.multiple_of((source * 2 + t) * row_count, row_count)
         return rows.at[pl.ds(start, row_count)]
 
-    late = row_count * 3 // 8
+    late = row_count // 4
     early = row_count - late
 
     def row_early(source):
@@ -301,14 +319,27 @@
 
     pair = 2 * hidden_piece
 
-    def guest_send(place):
-        start = pl.multiple_of((place * 2 + 1 - inner) * pair, 16)
-        spot = pl.ds(place * pair, pair)
+    low = outer < depth // 2
+    near = jnp.where(low, 1, 2 * depth - 3) - outer
+    at_end = (outer == 0) | (outer == depth - 1)
+
+    def direct(place, t):
+        return False
+
+    def unless(condition, action):
+        if condition is False:
+            action()
+        else:
+            pl.when(jnp.logical_not(condition))(action)
+
+    def guest_send(place, t):
+        e = (place * 2 + 1 - inner) * 2 + t
+        spot = pl.ds(place * pair + t * hidden_piece, hidden_piece)
         return remote(
-            pieces.at[:, pl.ds(start, pair), :],
+            piece(e),
             guests.at[:, spot, :],
-            guest_out_sem.at[place],
-            guest_sem.at[place],
+            guest_out_sem.at[place, t],
+            guest_sem.at[place, t],
             beside,
         )
 
@@ -340,8 +371,15 @@
             across,
         )
 
+    def with_table(block, source, t, send, recv, device):
+        entry = table.at[source * 2 + t]
+        return Both(
+            remote(block, block, send.at[0], recv.at[0], device),
+            remote(entry, entry, send.at[1], recv.at[1], device),
+        )
+
     def row_move(source, send, recv, device):
-        return remote(row_block(source, tp), row_block(source, tp), send, recv, device)
+        return with_table(row_block(source, tp), source, tp, send, recv, device)
 
     def row_onward(source, step):
         return row_move(
@@ -353,7 +391,9 @@
 
     def row_beside(source, distance):
         block = row_early(source) if distance < depth - 1 else row_block(source, tp)
-        return remote(block, block, row_side_sem.at[lax.div(source, 2)], row_sem.at[source], beside)
+        return with_table(
+            block, source, tp, row_side_sem.at[lax.div(source, 2)], row_sem.at[source], beside
+        )
 
     def mixed(place, send, step):
         block = row_late(place * 2 + 1 - inner)
@@ -408,7 +448,7 @@
 
     lane = lax.broadcasted_iota(jnp.int32, select.shape, 0)
     unit = lax.broadcasted_iota(jnp.int32, select.shape, 1)
-    first = (jnp.where(lane < LANES // 2, lane, lane - LANES // 2) - tp * n) * hidden_piece
+    first = (jnp.where(lane < 2 * n, lane, lane - 2 * n) - tp * n) * hidden_piece
     inside = (unit >= first) & (unit < first + hidden_piece) & (unit < hidden)
     select[...] = jnp.where(inside, 1.0, 0.0).astype(select.dtype)
     shared_far = remote(
@@ -485,7 +525,8 @@
 
     row_relay(outer * 2 + 1 - inner).start()
     for place in range(depth):
-        guest_send(place).start()
+        for t in range(2):
+            unless(direct(place, t), guest_send(place, t).start)
     for copy in locals_:
         copy.wait()
     far_columns = shared.at[:, :, columns(1 - gr, tp)]
@@ -494,6 +535,7 @@
     shared_relay.start()
     at_distance(2, arrive)
     ship(range(1, depth - 1))
+
     at_distance(1, arrive_mixed)
     at_distance(1, arrive_beside)
     at_distance(3, arrive)
@@ -501,12 +543,16 @@
     ship((0, depth - 1))
 
     for place in range(depth):
-        guest_send(place).wait_recv()
-
-        @pl.when(place != outer)
-        def _():
-            guest_onward(place, 0).start()
-            guest_onward(place, 1).start()
+        for t in range(2):
+
+            def onward(place=place, t=t):
+                guest_send(place, t).wait_recv()
+
+                @pl.when(place != outer)
+                def _():
+                    guest_onward(place, t).start()
+
+            unless(direct(place, t), onward)
 
     guest_onward(outer, other).start()
     guest_local.start()
@@ -552,10 +598,6 @@
             part_recv_sem.at[k],
             twin,
         )
-
-    low = outer < depth // 2
-    near = jnp.where(low, 1, 2 * depth - 3) - outer
-    at_end = (outer == 0) | (outer == depth - 1)
 
     def place_of(j):
         far = jnp.where(low, depth // 2 + j, depth // 2 - 1 - j)
@@ -666,15 +708,14 @@
         def _():
             at_distance(3, arrive_beside)
 
-        remote(
-            row_block(d, other), row_block(d, other), row_pair_out_sem.at[d], row_pair_sem.at[d], twin
+        with_table(
+            row_block(d, other), d, other, row_pair_out_sem.at[d], row_pair_sem.at[d], twin
         ).wait_recv()
         block = pl.ds(pl.multiple_of(d * 2 * row_count, 2 * row_count), 2 * row_count)
-        inputs = rows[block, 0:features]
+        inputs = rows[block, :]
+        entries = [table[d * 2 + t].astype(jnp.float32).T.astype(jnp.bfloat16) for t in range(2)]
         scale = jnp.dot(
-            rows[block, features : features + LANES],
-            select[...],
-            preferred_element_type=jnp.float32,
+            jnp.concatenate(entries, axis=0), select[...], preferred_element_type=jnp.float32
         )
         gate = contract_rows(inputs, weights[0])
         up = contract_rows(inputs, weights[1])
@@ -704,15 +745,16 @@
             take_weights(nearby(4))
             take_weights(nearby(6))
 
+        for h in range(steps):
+
+            @pl.when((k == n - 5 + 2 * h // steps) & at_end)
+            def _():
+                pass_far(0, h)
+
         @pl.when((k > depth) & (k < n - 1))
         def _():
             take_weights(nearby(2 * (k - depth) + 1))
 
-        for h in range(steps):
-
-            @pl.when((k == n - 4 + 2 * h // steps) & at_end)
-            def _():
-                pass_far(0, h)
 
     @pl.when(jnp.logical_not(at_end))
     def _():
@@ -803,15 +845,23 @@
         column_send(d).wait_send()
         row_relay(d).wait_send()
     for place in range(depth):
-        guest_send(place).wait_send()
-
-        @pl.when(place != outer)
-        def _():
-            for t in range(2):
+        for t in range(2):
+
+            def done(place=place, t=t):
+                guest_send(place, t).wait_send()
+
+                @pl.when(place != outer)
+                def _():
+                    guest_onward(place, t).wait_send()
+
+            unless(direct(place, t), done)
+
+            @pl.when(place != outer)
+            def _():
                 piece_send(place * 2 + inner, t).wait_send()
-                guest_onward(place, t).wait_send()
 
     guest_onward(outer, other).wait_send()
+
     for k in range(n):
         part_send(k).wait_send()
     for h in range(steps):
@@ -855,8 +905,9 @@
         out_specs=(vmem,) * 3,
         scratch_shapes=[
             pltpu.VMEM((3, hidden_all, features), kind),
-            pltpu.VMEM((experts * row_count, features + LANES), kind),
-            pltpu.VMEM((LANES, hidden_all), kind),
+            pltpu.VMEM((experts * row_count, features), kind),
+            pltpu.VMEM((experts, 2 * experts, row_count), kind),
+            pltpu.VMEM((2 * experts, hidden_all), kind),
             pltpu.VMEM((row_count, features), kind),
             pltpu.VMEM(routes.shape[::-1], jnp.int32),
             pltpu.VMEM(routes.shape[::-1], jnp.float32),
@@ -876,23 +927,23 @@
             DMA((3,)),
             DMA((3,)),
             DMA((n, 2)),
-            DMA((n // 2,)),
-            DMA((n // 2,)),
+            DMA((n // 2, 2)),
+            DMA((n // 2, 2)),
             DMA((n // 2, 2)),
             DMA((n, 2)),
             DMA((n,)),
             DMA((n,)),
             DMA((3,)),
             DMA((3,)),
-            DMA((n,)),
-            DMA((n // 2,)),
-            DMA((1,)),
-            DMA((n,)),
+            DMA((n, 2)),
+            DMA((n // 2, 2)),
+            DMA((1, 2)),
+            DMA((n, 2)),
             DMA((n // 2,)),
             DMA((1,)),
             DMA((n // 2,)),
-            DMA((n,)),
-            DMA((n,)),
+            DMA((n, 2)),
+            DMA((n, 2)),
             DMA((n,)),
             DMA((n,)),
             DMA((n // 2, 2)),

time: 128 us -> 125 us (0.977)
  Pallas kernels: 126 us -> 124 us
    pallas_call x1, Pallas kernels: 124 us -> 121 us  [direct_body(): pl.pallas_call(functools.partial(exchange_kernel, n), out_shape=(jax.Shap...]
where the time goes in v5:
time: 125 us
  Pallas kernels  124 us (99%)
    pallas_call x1, Pallas kernels, direct_body(): pl.pallas_call(functools.partial(exchange_kernel, n), out_shape=(jax.Shap...  121 us
    pallas_call x1, Pallas kernels, settle(): pl.pallas_call(settle_kernel, out_shape=(jax.ShapeDtypeStruct(combined.sh...  2.62 us

profile of v5, /device:TPU:0, one launch (start us, length us, event | category | flops | bytes accessed | tf_op | source)
XLA Modules:
  0.0 124.7 jit_solution(15067316189598995954)
XLA Ops:
  0.6 121.5 %shard_map.153 = (bf16[128,2048]{1,0:T(8,128)(2,1)S(1)}, bf16[3,384,2048]{2,1,0:T(8,128)(2,1)S(1)}, bf16[3,64,2048]{2,1,0:T(8,128)(2,1)S(1)}) custom-call(bf16[128,2048]{1,0:T(8,128)(2,1)} %tokens_hbm.1, s32[8,128]{1,0:T(8,128)} %bitcast.9, f32[8,128]{1,0:T(8,128)} %bitcast.10, f32[1,512]{1,0:T(1,128)} %bitcast.11, f32[768,512]{1,0:T(8,128)} %bitcast.6, ...), custom_call_target="tpu_custom_call" | custom-call | tf_op jit(solution)/shard_map/pallas_call | solution.py:897
  122.1 2.6 %shard_map.154 = (bf16[128,2048]{1,0:T(8,128)(2,1)}, bf16[1,384,2048]{2,1,0:T(8,128)(2,1)}, bf16[1,384,2048]{2,1,0:T(8,128)(2,1)}, bf16[1,384,2048]{2,1,0:T(8,12...) custom-call(bf16[128,2048]{1,0:T(8,128)(2,1)S(1)} %get-tuple-element.10.combined_ref, ...), custom_call_target="tpu_custom_call" | custom-call | tf_op jit(solution)/shard_map/pallas_call | solution.py:993

commit v6 on v5

--- a/solution.py
+++ b/solution.py
@@ -285,7 +285,7 @@
         start = pl.multiple_of((source * 2 + t) * row_count, row_count)
         return rows.at[pl.ds(start, row_count)]
 
-    late = row_count // 4
+    late = row_count * 3 // 8
     early = row_count - late
 
     def row_early(source):
@@ -736,14 +736,9 @@
                 add_pair(item - 1, h)
                 side_send(j, h).start()
 
-        @pl.when(k == 1)
+        @pl.when((k > 1) & (k <= depth))
         def _():
-            take_weights(nearby(2))
-
-        @pl.when(k == 2)
-        def _():
-            take_weights(nearby(4))
-            take_weights(nearby(6))
+            take_weights(nearby(2 * k - 2))
 
         for h in range(steps):
 
@@ -751,17 +746,19 @@
             def _():
                 pass_far(0, h)
 
-        @pl.when((k > depth) & (k < n - 1))
+        @pl.when((k > depth) & (k < n - 1) & at_end)
         def _():
             take_weights(nearby(2 * (k - depth) + 1))
 
 
     @pl.when(jnp.logical_not(at_end))
     def _():
+        take_weights(nearby(3))
         pass_near(2)
-        take_weights(nearby(n - 1))
         for h in range(steps):
             pass_far(0, h)
+        for i in range(2, depth):
+            take_weights(nearby(2 * i + 1))
 
     for h in range(steps):
         pass_far(1, h)

time: 125 us -> 124 us (level)
  no operation moved by 1% of the time
where the time goes in v6:
time: 124 us
  Pallas kernels  123 us (99%)
    pallas_call x1, Pallas kernels, direct_body(): pl.pallas_call(functools.partial(exchange_kernel, n), out_shape=(jax.Shap...  121 us
    pallas_call x1, Pallas kernels, settle(): pl.pallas_call(settle_kernel, out_shape=(jax.ShapeDtypeStruct(combined.sh...  2.62 us

profile of v6, /device:TPU:0, one launch (start us, length us, event | category | flops | bytes accessed | tf_op | source)
XLA Modules:
  0.0 123.8 jit_solution(8691053757792768321)
XLA Ops:
  0.6 120.6 %shard_map.153 = (bf16[128,2048]{1,0:T(8,128)(2,1)S(1)}, bf16[3,384,2048]{2,1,0:T(8,128)(2,1)S(1)}, bf16[3,64,2048]{2,1,0:T(8,128)(2,1)S(1)}) custom-call(bf16[128,2048]{1,0:T(8,128)(2,1)} %tokens_hbm.1, s32[8,128]{1,0:T(8,128)} %bitcast.9, f32[8,128]{1,0:T(8,128)} %bitcast.10, f32[1,512]{1,0:T(1,128)} %bitcast.11, f32[768,512]{1,0:T(8,128)} %bitcast.6, ...), custom_call_target="tpu_custom_call" | custom-call | tf_op jit(solution)/shard_map/pallas_call | solution.py:894
  121.2 2.6 %shard_map.154 = (bf16[128,2048]{1,0:T(8,128)(2,1)}, bf16[1,384,2048]{2,1,0:T(8,128)(2,1)}, bf16[1,384,2048]{2,1,0:T(8,128)(2,1)}, bf16[1,384,2048]{2,1,0:T(8,12...) custom-call(bf16[128,2048]{1,0:T(8,128)(2,1)S(1)} %get-tuple-element.10.combined_ref, ...), custom_call_target="tpu_custom_call" | custom-call | tf_op jit(solution)/shard_map/pallas_call | solution.py:990
